TPU v7x, 128 devices: a whole 4x4x4 slice. The times are simulated.
128 devices in a mesh: rep: 2 (over z_hi), fs: 32 (over z_lo, y, x), tp: 2 (over core).
Axes of the slice: x: 4, y: 4, z: 4 (z_hi: 2, z_lo: 2; z = z_hi * 2 + z_lo), core: 2. Of those that a mesh axis runs over, the one named last changes fastest.
Arguments:
- residual: bfloat16 [32768, 2048], P(('rep', 'fs', 'tp')), may hold values from -6 to 6
- mixer_gain: float32 [2048], replicated, may hold values from 0.1 to 1.9
- gating_proj: bfloat16 [2048, 2048], P('fs', 'tp'), may hold values from -0.125 to 0.125
- spatial_proj: bfloat16 [2048, 2048], P('fs', 'tp'), as said below
- spatial_gain: float32 [2048], replicated, may hold values from 0.1 to 1.9
- spatial_bias: float32 [2048], replicated, may hold values from -3 to 3
- spatial_mix: bfloat16 [32, 128, 128], replicated, may hold values from -0.5 to 0.5
- spatial_offset: float32 [32, 128], replicated, may hold values from 0.5 to 1.5
- mixer_out: bfloat16 [2048, 2048], P('tp', 'fs'), may hold values from -0.125 to 0.125
- channel_gain: float32 [2048], replicated, may hold values from 0.1 to 1.9
- gate_proj: bfloat16 [2048, 2816], P('fs', 'tp'), may hold values from -0.125 to 0.125
- up_proj: bfloat16 [2048, 2816], P('fs', 'tp'), may hold values from -0.125 to 0.125
- conv_taps: float32 [3, 2816], replicated, may hold values from -3.5 to 3.5
- down_proj: bfloat16 [2816, 2048], P('tp', 'fs'), may hold values from -0.109375 to 0.109375
Outputs:
- layer_out: bfloat16 [32768, 2048], P(('rep', 'fs', 'tp'))
Inputs may be any that keep to these rules, and one draw needn't show every extreme that they name: `spatial_proj`: entries are bounded in magnitude by 56 / sqrt(2048).
All inputs are finite; a program needn't handle non-finite values.
Results may differ from a plain program's by a relative error of at most 0.015.
Values may be sent and summed in bfloat16 or wider, within the bound.
No kernel may reach another device: no remote copies, remote signals or barrier semaphores. Data moves between devices by JAX's collectives and lax.ppermute only.
A program may use at most 128 MiB of HBM per device.

v0:
```python
import functools

import jax
import jax.numpy as jnp
from jax import lax
from jax.experimental import pallas as pl
from jax.experimental.pallas import tpu as pltpu
from jax.sharding import Mesh
from jax.sharding import PartitionSpec as P


D = 2048
HEAD = 64
GROUP = 2048
BLOCK = 128
SEGMENT = 64
SEQ = 256
QM = 512
QC = 768
QSTEP = 640
UNITS = 1408
FS = ("fs_0", "fs_1", "fs_2")
REP_FS_TP = ("rep", "fs_0", "fs_1", "fs_2", "tp")
Z = ("rep", "fs_0")
ZT = ("rep", "fs_0", "tp")
YXT = ("fs_1", "fs_2", "tp")
F32 = jnp.float32
BF16 = jnp.bfloat16


def ring(value, axis, by):
    return lax.ppermute(value, axis, [(i, (i + by) % 4) for i in range(4)])


def other_core(value):
    return lax.ppermute(value, "tp", [(0, 1), (1, 0)])


def to_partner(value):
    pairs = []
    for z in range(4):
        pairs.append((2 * z, 2 * ((z - 1) % 4)))
        pairs.append((2 * z + 1, 2 * ((z + 1) % 4) + 1))
    return lax.ppermute(value, ZT, pairs)


def to_owner(value):
    pairs = []
    for z in range(4):
        pairs.append((2 * z, 2 * ((z + 1) % 4)))
        pairs.append((2 * z + 1, 2 * ((z - 1) % 4) + 1))
    return lax.ppermute(value, ZT, pairs)


def along(value, first, by):
    pairs = []
    for y in range(4):
        for x in range(4):
            for t in range(2):
                on_x = (t == 0) == first
                to_x = (x + by) % 4 if on_x else x
                to_y = y if on_x else (y + by) % 4
                pairs.append((y * 8 + x * 2 + t, to_y * 8 + to_x * 2 + t))
    return lax.ppermute(value, YXT, pairs)


def plane_first(piece, route):
    back = along(piece, True, 1)
    ahead = along(piece, True, -1)
    return (piece, ahead, furthest(piece, ahead, back, True, route), back)


def furthest(piece, ahead, back, first, route):
    if route == 0:
        return along(piece, first, 2)
    return along(back, first, 1) if route > 0 else along(ahead, first, -1)


def join_kernel(widths, *refs):
    pieces, outs, sems = refs[:8], refs[8:-1], refs[-1]
    copies = []
    column = 0
    for k, width in enumerate(widths):
        for n, piece in enumerate(pieces):
            copies.append(
                pltpu.make_async_copy(
                    piece.at[:, pl.ds(column, width)], outs[k].at[pl.ds(n * 64, 64), :], sems.at[k * 8 + n]
                )
            )
        column += width
    for c in copies:
        c.start()
    for c in copies:
        c.wait()


def joined(pieces, widths):
    return pl.pallas_call(
        functools.partial(join_kernel, widths),
        out_shape=[jax.ShapeDtypeStruct((512, w), BF16) for w in widths],
        in_specs=[AN] * 8,
        out_specs=[VM] * len(widths),
        scratch_shapes=[pltpu.SemaphoreType.DMA((8 * len(widths),))],
        cost_estimate=pl.CostEstimate(flops=1 << 20, bytes_accessed=4 << 20, transcendentals=0),
        compiler_params=pltpu.CompilerParams(vmem_limit_bytes=6 << 20),
    )(*pieces)


def plane_second(line, route):
    back = along(line, False, 1)
    ahead = along(line, False, -1)
    return (line, ahead, furthest(line, ahead, back, False, route), back)


PLACES = [(s, f * 128 + h * 64, f, s, h) for s in range(4) for f in range(4) for h in range(2)]


def place_weight(refs, held):
    x = lax.axis_index("fs_2")
    y = lax.axis_index("fs_1")
    a = lax.axis_index("fs_0")
    t = lax.axis_index("tp")
    for which, row, first, second, half in PLACES:
        dx = first + t * (second - first)
        dy = second + t * (first - second)
        block = lax.rem(a + half, 2) * 16 + lax.rem(y + dy, 4) * 4 + lax.rem(x + dx, 4)
        held[pl.ds(pl.multiple_of(block * 64, 64), 64), :] = refs[which][row : row + 64, :]


def rms_normed(value, gain):
    wide = value.astype(F32)
    scale = lax.rsqrt(jnp.mean(wide * wide, axis=-1, keepdims=True) + 1e-06)
    return (wide * scale * gain).astype(BF16)


def norm_kernel(rows_in, gain, out):
    @pl.loop(0, SEQ // 32)
    def _(k):
        rows = pl.ds(pl.multiple_of(k * 32, 32), 32)
        out[rows, :] = rms_normed(rows_in[rows, :], gain[...])


def as_row(column):
    return jnp.broadcast_to(column, (BLOCK, BLOCK)).T[0:1, :]


def as_column(row):
    return jnp.broadcast_to(row, (BLOCK, BLOCK)).T


def spatial_kernel(own, own2, rem, rem2, *rest):
    pieces, (act_v, sums), (held,) = rest[:4], rest[4:6], rest[6:]
    t = lax.axis_index("tp")
    place_weight(pieces, held)
    for s, ref in enumerate((own, own2, rem, rem2)):
        v = jnp.dot(ref[...], held[...], preferred_element_type=F32)
        v = jax.nn.gelu(v.astype(BF16).astype(F32))
        act_v[s * SEQ : (s + 1) * SEQ, :] = v
        place = 2 * (s // 2) + lax.rem(s + t, 2)
        total = jnp.sum(v, axis=-1, keepdims=True)
        squares = jnp.sum(v * v, axis=-1, keepdims=True)
        for b in range(2):
            part = slice(b * BLOCK, (b + 1) * BLOCK)
            sums[place, b : b + 1, :] = as_row(total[part])
            sums[place, 2 + b : 3 + b, :] = as_row(squares[part])


def gating_kernel(own, own2, rem, rem2, *rest):
    pieces, (act_u,), (held,) = rest[:4], rest[4:5], rest[5:]
    place_weight(pieces, held)
    for s, ref in enumerate((own, own2, rem, rem2)):
        u = jnp.dot(ref[...], held[...], preferred_element_type=F32)
        act_u[s * SEQ : (s + 1) * SEQ, :] = jax.nn.gelu(u.astype(BF16).astype(F32))


def mix_kernel(pair, act_u, act_v, sums, gain, bias, offset, mix_all, *rest):
    pieces, outs, (held, gated, mix, shift) = rest[:4], rest[4:6], rest[6:]
    t = lax.axis_index("tp")
    a = lax.axis_index("fs_0")
    place_weight(pieces, held)
    start = pl.multiple_of(t * 1024 + a * QM, QM)
    gains = gain[:, pl.ds(start, QM)]
    biases = bias[:, pl.ds(start, QM)]
    lane = lax.broadcasted_iota(jnp.int32, (BLOCK, 128), 1)
    first_head = pl.multiple_of(t * 16 + a * 8, 8)
    offsets = offset[pl.ds(first_head, 8), :]
    for c in range(QM // 128):
        one, two = as_column(offsets[2 * c : 2 * c + 1]), as_column(offsets[2 * c + 1 : 2 * c + 2])
        shift[:, c * 128 : (c + 1) * 128] = jnp.where(lane < HEAD, one, two)
    allowed = lane // SEGMENT <= lax.broadcasted_iota(jnp.int32, (BLOCK, BLOCK), 0) // SEGMENT
    for h in range(8):
        mix[h] = jnp.where(allowed, mix_all[first_head + h].astype(F32), 0.0).astype(BF16)

    @pl.loop(0, 2)
    def _(s):
        place = 2 * pair + lax.rem(s + t, 2)
        for b in range(2):
            here = s * SEQ + b * BLOCK
            rows = pl.ds(pl.multiple_of(2 * pair * SEQ + here, BLOCK), BLOCK)
            to = pl.ds(pl.multiple_of(here, BLOCK), BLOCK)
            mean = as_column(sums[place, b : b + 1, :]) / GROUP
            var = as_column(sums[place, 2 + b : 3 + b, :]) / GROUP - mean * mean
            scale = lax.rsqrt(var + 1e-05)
            for c in range(QM // 128):
                lanes = slice(c * 128, (c + 1) * 128)
                v = (act_v[rows, lanes] - mean) * scale * gains[:, lanes] + biases[:, lanes]
                v = v.astype(BF16)
                one = jnp.dot(mix[2 * c], v, preferred_element_type=F32)
                two = jnp.dot(mix[2 * c + 1], v, preferred_element_type=F32)
                mixed = jnp.where(lane < HEAD, one, two) + shift[:, lanes]
                gated[to, lanes] = (act_u[rows, lanes] * mixed).astype(BF16)

    for s in (1, 0):
        out = lax.dot_general(
            gated[s * SEQ : (s + 1) * SEQ, :], held[...], (((1,), (1,)), ((), ())), preferred_element_type=F32
        )
        outs[s][...] = out.astype(BF16)


def assemble_kernel(*refs):
    n = len(refs) // 5
    for k in range(n):
        place_weight(refs[4 * k : 4 * k + 4], refs[4 * n + k])


def hidden_kernel(first, second, wgate, wup, taps_all, hidden):
    a = lax.axis_index("fs_0")
    t = lax.axis_index("tp")
    taps = taps_all[:, pl.ds(pl.multiple_of(t * UNITS + a * QSTEP, 128), QC)]
    for s, ref in enumerate((first, second)):
        gate = jnp.dot(ref[...], wgate[...], preferred_element_type=F32).astype(BF16).astype(F32)
        up = jnp.dot(ref[...], wup[...], preferred_element_type=F32).astype(BF16).astype(F32)
        row = lax.broadcasted_iota(jnp.int32, gate.shape, 0)
        conv = taps[2:3, :] * gate
        for lag in (1, 2):
            conv = conv + taps[2 - lag : 3 - lag, :] * jnp.where(row >= lag, pltpu.roll(gate, lag, 0), 0.0)
        product = jax.nn.silu(conv) * up
        lane = lax.broadcasted_iota(jnp.int32, gate.shape, 1)
        hidden[s] = jnp.where(lane >= 128 * a, product, 0.0).astype(BF16)


def down_kernel(hidden, wdown, out_first, out_second):
    for s, out_ref in ((1, out_second), (0, out_first)):
        out = lax.dot_general(hidden[s], wdown[...], (((1,), (1,)), ((), ())), preferred_element_type=F32)
        out_ref[...] = out.astype(BF16)


VM = pl.BlockSpec(memory_space=pltpu.VMEM)
AN = pl.BlockSpec(memory_space=pltpu.HBM)


def call(kernel, out_shape, scratch, flops, limit, args):
    return pl.pallas_call(
        kernel,
        out_shape=out_shape,
        in_specs=[VM] * len(args),
        out_specs=jax.tree.map(lambda _: VM, out_shape),
        scratch_shapes=scratch,
        cost_estimate=pl.CostEstimate(flops=int(flops), bytes_accessed=8 << 20, transcendentals=0),
        compiler_params=pltpu.CompilerParams(vmem_limit_bytes=limit << 20),
    )(*args)


def plus_kernel(n, gained, *refs):
    @pl.loop(0, SEQ // 32)
    def _(k):
        rows = pl.ds(pl.multiple_of(k * 32, 32), 32)
        total = refs[0][rows, :].astype(F32)
        for ref in refs[1:n]:
            total = total + ref[rows, :].astype(F32)
        total = total.astype(BF16)
        if gained:
            refs[n + 1][rows, :] = total
            refs[n + 2][rows, :] = rms_normed(total, refs[n][...])
        else:
            refs[n][rows, :] = total


def plus(*arrays, gain=None):
    one = jax.ShapeDtypeStruct((SEQ, D), BF16)
    args = arrays if gain is None else (*arrays, gain)
    return pl.pallas_call(
        functools.partial(plus_kernel, len(arrays), gain is not None),
        out_shape=one if gain is None else (one, one),
        in_specs=[VM] * len(args),
        out_specs=VM if gain is None else (VM, VM),
        cost_estimate=pl.CostEstimate(flops=1 << 20, bytes_accessed=4 << 20, transcendentals=0),
        compiler_params=pltpu.CompilerParams(vmem_limit_bytes=10 << 20),
    )(*args)


def normed(rows, gain):
    return pl.pallas_call(
        norm_kernel,
        out_shape=jax.ShapeDtypeStruct((SEQ, D), BF16),
        in_specs=[VM, VM],
        out_specs=VM,
        cost_estimate=pl.CostEstimate(flops=1 << 20, bytes_accessed=2 << 20, transcendentals=0),
        compiler_params=pltpu.CompilerParams(vmem_limit_bytes=6 << 20),
    )(rows, gain)


def arr(shape, dtype):
    return jax.ShapeDtypeStruct(shape, dtype)


def on_device(
    residual,
    mixer_gain,
    gating_proj,
    spatial_proj,
    spatial_gain,
    spatial_bias,
    spatial_mix,
    spatial_offset,
    mixer_out,
    channel_gain,
    gate_proj,
    up_proj,
    conv_taps,
    down_proj,
):
    a = lax.axis_index("fs_0")

    def window(arrays, which, step, width):
        return jnp.concatenate(
            [lax.dynamic_slice_in_dim(w, which * step, width, 1) for w in arrays], axis=1
        )

    mixer_arrays = (spatial_proj, gating_proj, mixer_out.T)
    channel_arrays = (gate_proj, up_proj, down_proj.T)

    def first_phase(arrays, step, width, by, routes):
        give = window(arrays, 1 - a, step, width)
        mine = window(arrays, a, step, width)
        theirs = ring(give, Z, by)
        firsts = zip(plane_first(mine, routes[0]), plane_first(theirs, routes[1]))
        return [piece for both in firsts for piece in both]

    own = residual
    rem = to_partner(own)
    own_n = normed(own, mixer_gain[None])
    own2_n = other_core(own_n)
    rem_n = normed(rem, mixer_gain[None])
    rem2_n = other_core(rem_n)
    m_first = first_phase(mixer_arrays, QM, QM, 1, (0, 0))
    s_line, u_line, o_line = joined(m_first, (QM,) * 3)
    s_pieces = plane_second(s_line, 1)
    u_pieces = plane_second(u_line, -1)
    o_pieces = plane_second(o_line, 0)
    c_first = first_phase(channel_arrays, QSTEP, QC, -1, (1, -1))
    g_line, h_line, d_line = joined(c_first, (QC,) * 3)
    g_pieces = plane_second(g_line, 1)
    h_pieces = plane_second(h_line, -1)
    d_pieces = plane_second(d_line, 0)
    seqs = (own_n, own2_n, rem_n, rem2_n)

    act_v, sums = call(
        spatial_kernel,
        (arr((4 * SEQ, QM), F32), arr((4, 4, 128), F32)),
        [pltpu.VMEM((D, QM), BF16)],
        2 * 1024 * D * QM,
        14,
        (*seqs, *s_pieces),
    )
    sums = sums + other_core(sums)
    from_below = ring(sums[1:3], Z, 1)
    from_above = ring(jnp.stack([sums[0], sums[3]]), Z, -1)
    sums = sums + jnp.stack([from_below[1], from_above[1], from_above[0], from_below[0]])
    (act_u,) = call(
        gating_kernel,
        (arr((4 * SEQ, QM), F32),),
        [pltpu.VMEM((D, QM), BF16)],
        2 * 1024 * D * QM,
        14,
        (*seqs, *u_pieces),
    )
    pair = (arr((SEQ, D), BF16),) * 2

    def mixed(k):
        return call(
            functools.partial(mix_kernel, k),
            pair,
            [pltpu.VMEM((D, QM), BF16), pltpu.VMEM((2 * SEQ, QM), BF16), pltpu.VMEM((8, 128, 128), BF16)]
            + [pltpu.VMEM((128, QM), F32)],
            1024 * D * QM,
            16,
            (act_u, act_v, sums, spatial_gain[None], spatial_bias[None], spatial_offset, spatial_mix, *o_pieces),
        )

    part, part2 = mixed(0)
    s_own = plus(part, other_core(part2))
    part, part2 = mixed(1)
    s_rem = plus(part, other_core(part2))
    _, rem_n = plus(rem, s_rem, to_partner(s_own), gain=channel_gain[None])
    mid_own, own_n = plus(own, s_own, to_owner(s_rem), gain=channel_gain[None])
    rem2_n = other_core(rem_n)
    own2_n = other_core(own_n)

    def assembled(*groups):
        flat = [p for g in groups for p in g]
        return pl.pallas_call(
            assemble_kernel,
            out_shape=[arr((D, QC), BF16)] * len(groups),
            in_specs=[VM] * len(flat),
            out_specs=[VM] * len(groups),
            cost_estimate=pl.CostEstimate(flops=1 << 20, bytes_accessed=8 << 20, transcendentals=0),
            compiler_params=pltpu.CompilerParams(vmem_limit_bytes=16 << 20),
        )(*flat)

    wgate, wup = assembled(g_pieces, h_pieces)
    (wdown,) = assembled(d_pieces)

    def hid(first, second):
        (out,) = call(
            hidden_kernel, (arr((2, SEQ, QC), BF16),), [], 2 * 1024 * D * QC, 20, (first, second, wgate, wup, conv_taps)
        )
        return out

    def down(hidden):
        return call(down_kernel, pair, [], 1024 * D * QC, 14, (hidden, wdown))

    hidden_r = hid(rem_n, rem2_n)
    hidden_o = hid(own_n, own2_n)
    part, part2 = down(hidden_r)
    s_rem = plus(part, other_core(part2))
    part, part2 = down(hidden_o)
    return plus(mid_own, part, other_core(part2), to_owner(s_rem))


def solution(mesh):
    split = Mesh(
        mesh.devices.reshape(mesh.shape["rep"], 2, 4, 4, mesh.shape["tp"]),
        ("rep", "fs_0", "fs_1", "fs_2", "tp"),
    )
    placed = (
        P(REP_FS_TP, None),
        P(),
        P(FS, "tp"),
        P(FS, "tp"),
        P(),
        P(),
        P(),
        P(),
        P("tp", FS),
        P(),
        P(FS, "tp"),
        P(FS, "tp"),
        P(),
        P("tp", FS),
    )

    return jax.shard_map(on_device, mesh=split, in_specs=placed, out_specs=P(REP_FS_TP, None), check_vma=False)
```

profile of v0, /device:TPU:1, one launch (start us, length us, event | category | flops | bytes accessed | tf_op | source)
XLA Modules:
  0.0 187.6 jit_solution(962398422326387644)
XLA Ops:
  0.0 2.5 %collective-permute-start.1 = (bf16[256,2048]{1,0:T(8,128)(2,1)}, bf16[256,2048]{1,0:T(8,128)(2,1)S(1)}, u32[]{:S(2)}, u32[]{:S(2)}) collective-permute-start(bf16[256,2048]{1,0:T(8,128)(2,1)} %refs_0_.1), channel_id=1, source_target_pairs={{0,96},{1,33},{32,0},{33,65},{64,32},{65,97},{96,64},{97,1},{2,98}... | collective-permute-start | bytes 3145736 | tf_op jit(solution)/shard_map/ppermute | solution.py:44
  4.3 1.7 collective-permute-start.3
  6.1 2.8 %collective-permute-start.4 = (bf16[64,1536]{1,0:T(8,128)(2,1)S(1)}, bf16[64,1536]{1,0:T(8,128)(2,1)S(1)}, u32[]{:S(2)}, u32[]{:S(2)}) collective-permute-start(bf16[64,1536]{1,0:T(8,128)(2,1)S(1)} %pad_maximum_fusion.2.refs_0_), channel_id=1, source_target_pairs={{0,6},{1,25},{2,0},{3,27},{4,2},{5,29},{6,4},{7,31},{8,14},{9,1},{... | collective-permute-start | bytes 589832 | tf_op jit(solution)/shard_map/ppermute | solution.py:64
  9.9 11.3 %collective-permute-done.3.refs_1_ = bf16[64,1536]{1,0:T(8,128)(2,1)S(1)} collective-permute-done((bf16[64,1536]{1,0:T(8,128)(2,1)S(1)}, bf16[64,1536]{1,0:T(8,128)(2,1)S(1)}, u32[]{:S(2)}, u32[]{:S(2)}) %collective-permute-start.3) | collective-permute-done | bytes 196640 | tf_op jit(solution)/shard_map/ppermute | solution.py:32
  21.2 2.7 %collective-permute-start.5 = (bf16[64,1536]{1,0:T(8,128)(2,1)S(1)}, bf16[64,1536]{1,0:T(8,128)(2,1)S(1)}, u32[]{:S(2)}, u32[]{:S(2)}) collective-permute-start(bf16[64,1536]{1,0:T(8,128)(2,1)S(1)} %collective-permute-done.3.refs_1_), channel_id=1, source_target_pairs={{0,6},{1,25},{2,0},{3,27},{4,2},{5,29},{6,4},{7,31},{8,14},{9,1},{... | collective-permute-start | bytes 589832 | tf_op jit(solution)/shard_map/ppermute | solution.py:64
  25.0 1.2 copy-done
  28.6 1.4 collective-permute-done.7.refs_5_
  30.0 2.0 %collective-permute-done.9.refs_7_ = bf16[64,1536]{1,0:T(8,128)(2,1)S(1)} collective-permute-done((bf16[64,1536]{1,0:T(8,128)(2,1)S(1)}, bf16[64,1536]{1,0:T(8,128)(2,1)S(1)}, u32[]{:S(2)}, u32[]{:S(2)}) %collective-permute-start.9) | collective-permute-done | bytes 196640 | tf_op jit(solution)/shard_map/ppermute | solution.py:64
  32.1 1.5 shard_map.138
  36.7 1.6 collective-permute-start.13
  38.3 1.5 collective-permute-start.10
  39.8 4.2 %collective-permute-done.14.rest_3_ = bf16[512,512]{1,0:T(8,128)(2,1)} collective-permute-done((bf16[512,512]{1,0:T(8,128)(2,1)}, bf16[512,512]{1,0:T(8,128)(2,1)}, u32[]{:S(2)}, u32[]{:S(2)}) %collective-permute-start.14) | collective-permute-done | bytes 524320 | tf_op jit(solution)/shard_map/ppermute | solution.py:64
  45.4 1.2 collective-permute-start.12
  46.6 4.4 %collective-permute-done.10.rest_1_ = bf16[512,512]{1,0:T(8,128)(2,1)} collective-permute-done((bf16[512,512]{1,0:T(8,128)(2,1)}, bf16[512,512]{1,0:T(8,128)(2,1)}, u32[]{:S(2)}, u32[]{:S(2)}) %collective-permute-start.10) | collective-permute-done | bytes 524320 | tf_op jit(solution)/shard_map/ppermute | solution.py:64
  51.0 2.8 %collective-permute-start.11 = (bf16[512,512]{1,0:T(8,128)(2,1)}, bf16[512,512]{1,0:T(8,128)(2,1)S(1)}, u32[]{:S(2)}, u32[]{:S(2)}) collective-permute-start(bf16[512,512]{1,0:T(8,128)(2,1)} %collective-permute-done.10.rest_1_), channel_id=1, source_target_pairs={{0,24},{1,7},{2,26},{3,1},{4,28},{5,3},{6,30},{7,5},{8,0},{9,15},{... | collective-permute-start | bytes 1572872 | tf_op jit(solution)/shard_map/ppermute | solution.py:64
  53.8 5.4 %shard_map.140 = (f32[1024,512]{1,0:T(8,128)S(1)}, f32[4,4,128]{2,1,0:T(4,128)S(1)}) custom-call(bf16[256,2048]{1,0:T(8,128)(2,1)S(1)} %shard_map.136.own, bf16[256,2048]{1,0:T(8,128)(2,1)} %collective-permute-done.own2, bf16[256,2048]{1,0:T(8,128)(2,1)S(1)} %shard_map.137.rem, bf16[256,2048]{1,0:T(8,128)(2,1)} %collective-permute-done.2.rem2, ...), custom_call_target="tpu_custom_call" | custom-call | flops 2147483648 | bytes 8388608 | tf_op jit(solution)/shard_map/pallas_call | solution.py:253
  59.6 1.8 collective-permute-start.26
  62.6 1.8 collective-permute-start.20
  65.1 4.8 %shard_map.139.act_u = f32[1024,512]{1,0:T(8,128)S(1)} custom-call(bf16[256,2048]{1,0:T(8,128)(2,1)S(1)} %shard_map.136.own, bf16[256,2048]{1,0:T(8,128)(2,1)} %collective-permute-done.own2, bf16[256,2048]{1,0:T(8,128)(2,1)S(1)} %shard_map.137.rem, bf16[256,2048]{1,0:T(8,128)(2,1)} %collective-permute-done.2.rem2, ...), custom_call_target="tpu_custom_call" | custom-call | flops 2147483648 | bytes 8388608 | tf_op jit(solution)/shard_map/pallas_call | solution.py:253
  69.9 1.4 collective-permute-start.17
  71.3 2.7 %collective-permute-done.17 = f32[2,4,128]{2,1,0:T(4,128)S(1)} collective-permute-done((f32[2,4,128]{2,1,0:T(4,128)S(1)}, f32[2,4,128]{2,1,0:T(4,128)S(1)}, u32[]{:S(2)}, u32[]{:S(2)}) %collective-permute-start.17) | collective-permute-done | bytes 4128 | tf_op jit(solution)/shard_map/ppermute | solution.py:32
  74.0 4.1 %collective-permute-done.21.rest_3_ = bf16[512,512]{1,0:T(8,128)(2,1)S(1)} collective-permute-done((bf16[512,512]{1,0:T(8,128)(2,1)S(1)}, bf16[512,512]{1,0:T(8,128)(2,1)S(1)}, u32[]{:S(2)}, u32[]{:S(2)}) %collective-permute-start.21) | collective-permute-done | bytes 524320 | tf_op jit(solution)/shard_map/ppermute | solution.py:64
  78.1 2.5 %shard_map.141 = (bf16[256,2048]{1,0:T(8,128)(2,1)S(1)}, bf16[256,2048]{1,0:T(8,128)(2,1)S(1)}) custom-call(f32[1024,512]{1,0:T(8,128)S(1)} %shard_map.139.act_u, f32[1024,512]{1,0:T(8,128)S(1)} %get-tuple-element.28.act_v, f32[4,4,128]{2,1,0:T(4,128)S(1)} %maximum_add_fusion.sums, f32[1,2048]{1,0:T(1,128)S(1)} %bitcast.16, f32[1,2048]{1,0:T(1,128)S(1)} %bitcast.18, ...), custom_call_target="tpu_custom_call" | custom-call | flops 1073741824 | bytes 8388608 | tf_op jit(solution)/shard_map/pallas_call | solution.py:253
  81.3 2.5 %collective-permute-start.28 = (bf16[64,2304]{1,0:T(8,128)(2,1)S(1)}, bf16[64,2304]{1,0:T(8,128)(2,1)S(1)}, u32[]{:S(2)}, u32[]{:S(2)}) collective-permute-start(bf16[64,2304]{1,0:T(8,128)(2,1)S(1)} %collective-permute-done.26.refs_1_), channel_id=1, source_target_pairs={{0,6},{1,25},{2,0},{3,27},{4,2},{5,29},{6,4},{7,31},{8,14},{9,1},{... | collective-permute-start | bytes 884744 | tf_op jit(solution)/shard_map/ppermute | solution.py:64
  83.8 1.4 collective-permute-start.32
  85.3 2.9 %collective-permute-done.29.refs_6_ = bf16[64,2304]{1,0:T(8,128)(2,1)S(1)} collective-permute-done((bf16[64,2304]{1,0:T(8,128)(2,1)S(1)}, bf16[64,2304]{1,0:T(8,128)(2,1)S(1)}, u32[]{:S(2)}, u32[]{:S(2)}) %collective-permute-start.29) | collective-permute-done | bytes 294944 | tf_op jit(solution)/shard_map/ppermute | solution.py:64
  88.2 2.7 %collective-permute-start.31 = (bf16[64,2304]{1,0:T(8,128)(2,1)S(1)}, bf16[64,2304]{1,0:T(8,128)(2,1)S(1)}, u32[]{:S(2)}, u32[]{:S(2)}) collective-permute-start(bf16[64,2304]{1,0:T(8,128)(2,1)S(1)} %collective-permute-done.28.refs_3_), channel_id=1, source_target_pairs={{0,6},{1,25},{2,0},{3,27},{4,2},{5,29},{6,4},{7,31},{8,14},{9,1},{... | collective-permute-start | bytes 884744 | tf_op jit(solution)/shard_map/ppermute | solution.py:64
  90.9 2.4 %shard_map.143 = (bf16[256,2048]{1,0:T(8,128)(2,1)S(1)}, bf16[256,2048]{1,0:T(8,128)(2,1)S(1)}) custom-call(f32[1024,512]{1,0:T(8,128)S(1)} %shard_map.139.act_u, f32[1024,512]{1,0:T(8,128)S(1)} %get-tuple-element.28.act_v, f32[4,4,128]{2,1,0:T(4,128)S(1)} %maximum_add_fusion.sums, f32[1,2048]{1,0:T(1,128)S(1)} %bitcast.17, f32[1,2048]{1,0:T(1,128)S(1)} %bitcast.19, ...), custom_call_target="tpu_custom_call" | custom-call | flops 1073741824 | bytes 8388608 | tf_op jit(solution)/shard_map/pallas_call | solution.py:253
  93.4 1.6 collective-permute-start.23
  96.3 2.4 %collective-permute-start.36 = (bf16[512,768]{1,0:T(8,128)(2,1)S(1)}, bf16[512,768]{1,0:T(8,128)(2,1)S(1)}, u32[]{:S(2)}, u32[]{:S(2)}) collective-permute-start(bf16[512,768]{1,0:T(8,128)(2,1)S(1)} %get-tuple-element.38.refs_4_), channel_id=1, source_target_pairs={{0,24},{1,7},{2,26},{3,1},{4,28},{5,3},{6,30},{7,5},{8,0},{9,15},{... | collective-permute-start | bytes 2359304 | tf_op jit(solution)/shard_map/ppermute | solution.py:64
  99.2 9.2 %collective-permute-done.34.refs_3_ = bf16[512,768]{1,0:T(8,128)(2,1)S(1)} collective-permute-done((bf16[512,768]{1,0:T(8,128)(2,1)S(1)}, bf16[512,768]{1,0:T(8,128)(2,1)S(1)}, u32[]{:S(2)}, u32[]{:S(2)}) %collective-permute-start.34) | collective-permute-done | bytes 786464 | tf_op jit(solution)/shard_map/ppermute | solution.py:64
  109.6 2.1 %collective-permute-start.41 = (bf16[512,768]{1,0:T(8,128)(2,1)S(1)}, bf16[512,768]{1,0:T(8,128)(2,1)S(1)}, u32[]{:S(2)}, u32[]{:S(2)}) collective-permute-start(bf16[512,768]{1,0:T(8,128)(2,1)S(1)} %get-tuple-element.41.refs_0_), channel_id=1, source_target_pairs={{0,8},{1,3},{2,10},{3,5},{4,12},{5,7},{6,14},{7,1},{8,16},{9,11},{... | collective-permute-start | bytes 2359304 | tf_op jit(solution)/shard_map/ppermute | solution.py:64
  111.9 2.0 %collective-permute-done.43.refs_2_ = bf16[256,2048]{1,0:T(8,128)(2,1)S(1)} collective-permute-done((bf16[256,2048]{1,0:T(8,128)(2,1)S(1)}, bf16[256,2048]{1,0:T(8,128)(2,1)S(1)}, u32[]{:S(2)}, u32[]{:S(2)}) %collective-permute-start.43) | collective-permute-done | bytes 1048608 | tf_op jit(solution)/shard_map/ppermute | solution.py:44
  113.9 2.2 %shard_map.151 = (bf16[256,2048]{1,0:T(8,128)(2,1)}, bf16[256,2048]{1,0:T(8,128)(2,1)S(1)}) custom-call(bf16[256,2048]{1,0:T(8,128)(2,1)S(1)} %collective-permute-done.1.rows_in.refs_0_, bf16[256,2048]{1,0:T(8,128)(2,1)S(1)} %shard_map.144.refs_1_, bf16[256,2048]{1,0:T(8,128)(2,1)S(1)} %collective-permute-done.43.refs_2_, f32[1,2048]{1,0:T(1,128)S(1)} %bitcast.14), custom_call_target="tpu_custom_call" | custom-call | flops 1048576 | bytes 4194304 | tf_op jit(solution)/shard_map/pallas_call | solution.py:282
  116.2 2.9 %collective-permute-start.44 = (bf16[256,2048]{1,0:T(8,128)(2,1)S(1)}, bf16[256,2048]{1,0:T(8,128)(2,1)S(1)}, u32[]{:S(2)}, u32[]{:S(2)}) collective-permute-start(bf16[256,2048]{1,0:T(8,128)(2,1)S(1)} %get-tuple-element.44.first), channel_id=1, source_target_pairs={{0,1},{1,0},{2,3},{3,2},{4,5},{5,4},{6,7},{7,6},{8,9},{9,8},{10,11... | collective-permute-start | bytes 3145736 | tf_op jit(solution)/shard_map/ppermute | solution.py:36
  119.0 13.9 %collective-permute-done.39.refs_1_ = bf16[512,768]{1,0:T(8,128)(2,1)S(1)} collective-permute-done((bf16[512,768]{1,0:T(8,128)(2,1)S(1)}, bf16[512,768]{1,0:T(8,128)(2,1)S(1)}, u32[]{:S(2)}, u32[]{:S(2)}) %collective-permute-start.39) | collective-permute-done | bytes 786464 | tf_op jit(solution)/shard_map/ppermute | solution.py:64
  133.9 2.5 %collective-permute-start.37 = (bf16[512,768]{1,0:T(8,128)(2,1)S(1)}, bf16[512,768]{1,0:T(8,128)(2,1)S(1)}, u32[]{:S(2)}, u32[]{:S(2)}) collective-permute-start(bf16[512,768]{1,0:T(8,128)(2,1)S(1)} %collective-permute-done.36.refs_5_), channel_id=1, source_target_pairs={{0,24},{1,7},{2,26},{3,1},{4,28},{5,3},{6,30},{7,5},{8,0},{9,15},{... | collective-permute-start | bytes 2359304 | tf_op jit(solution)/shard_map/ppermute | solution.py:64
  136.7 9.3 %collective-permute-done.38.refs_7_ = bf16[512,768]{1,0:T(8,128)(2,1)S(1)} collective-permute-done((bf16[512,768]{1,0:T(8,128)(2,1)S(1)}, bf16[512,768]{1,0:T(8,128)(2,1)S(1)}, u32[]{:S(2)}, u32[]{:S(2)}) %collective-permute-start.38) | collective-permute-done | bytes 786464 | tf_op jit(solution)/shard_map/ppermute | solution.py:64
  146.0 8.4 %collective-permute-done.35.refs_2_ = bf16[512,768]{1,0:T(8,128)(2,1)S(1)} collective-permute-done((bf16[512,768]{1,0:T(8,128)(2,1)S(1)}, bf16[512,768]{1,0:T(8,128)(2,1)S(1)}, u32[]{:S(2)}, u32[]{:S(2)}) %collective-permute-start.35) | collective-permute-done | bytes 786464 | tf_op jit(solution)/shard_map/ppermute | solution.py:64
  154.9 1.4 shard_map.145
  156.3 3.6 %collective-permute-start.25 = (bf16[256,2048]{1,0:T(8,128)(2,1)S(1)}, bf16[256,2048]{1,0:T(8,128)(2,1)S(1)}, u32[]{:S(2)}, u32[]{:S(2)}) collective-permute-start(bf16[256,2048]{1,0:T(8,128)(2,1)S(1)} %get-tuple-element.36.first), channel_id=1, source_target_pairs={{0,1},{1,0},{2,3},{3,2},{4,5},{5,4},{6,7},{7,6},{8,9},{9,8},{10,11... | collective-permute-start | bytes 3145736 | tf_op jit(solution)/shard_map/ppermute | solution.py:36
  159.9 3.7 %shard_map.152.hidden = bf16[2,256,768]{2,1,0:T(8,128)(2,1)S(1)} custom-call(bf16[256,2048]{1,0:T(8,128)(2,1)S(1)} %get-tuple-element.44.first, bf16[256,2048]{1,0:T(8,128)(2,1)S(1)} %collective-permute-done.44.second, bf16[2048,768]{1,0:T(8,128)(2,1)S(1)} %get-tuple-element.39.wgate, bf16[2048,768]{1,0:T(8,128)(2,1)S(1)} %get-tuple-element.40.wup, ...), custom_call_target="tpu_custom_call" | custom-call | flops 3221225472 | bytes 8388608 | tf_op jit(solution)/shard_map/pallas_call | solution.py:253
  163.7 1.9 shard_map.153
  165.6 3.7 %shard_map.148.hidden = bf16[2,256,768]{2,1,0:T(8,128)(2,1)S(1)} custom-call(bf16[256,2048]{1,0:T(8,128)(2,1)S(1)} %get-tuple-element.36.first, bf16[256,2048]{1,0:T(8,128)(2,1)S(1)} %collective-permute-done.25.second, bf16[2048,768]{1,0:T(8,128)(2,1)S(1)} %get-tuple-element.39.wgate, bf16[2048,768]{1,0:T(8,128)(2,1)S(1)} %get-tuple-element.40.wup, ...), custom_call_target="tpu_custom_call" | custom-call | flops 3221225472 | bytes 8388608 | tf_op jit(solution)/shard_map/pallas_call | solution.py:253
  169.4 1.8 shard_map.150
  172.5 1.5 collective-permute-done.42.refs_2_
  174.1 12.0 %collective-permute-done.46.refs_3_ = bf16[256,2048]{1,0:T(8,128)(2,1)S(1)} collective-permute-done((bf16[256,2048]{1,0:T(8,128)(2,1)S(1)}, bf16[256,2048]{1,0:T(8,128)(2,1)S(1)}, u32[]{:S(2)}, u32[]{:S(2)}) %collective-permute-start.46) | collective-permute-done | bytes 1048608 | tf_op jit(solution)/shard_map/ppermute | solution.py:52
  186.1 1.5 shard_map.155
  (107 shorter events, 20.2 us)
Async XLA Ops:
  0.0 35.6 %collective-permute-start.1 = (bf16[256,2048]{1,0:T(8,128)(2,1)}, bf16[256,2048]{1,0:T(8,128)(2,1)S(1)}, u32[]{:S(2)}, u32[]{:S(2)}) collective-permute-start(bf16[256,2048]{1,0:T(8,128)(2,1)} %refs_0_.1), channel_id=1, source_target_pairs={{0,96},{1,33},{32,0},{33,65},{64,32},{65,97},{96,64},{97,1},{2,98}... | collective-permute-start | bytes 3145736 | tf_op jit(solution)/shard_map/ppermute | solution.py:44
  4.3 39.9 %copy-start.11 = (bf16[1408,64]{0,1:T(8,128)(2,1)S(1)}, bf16[1408,64]{0,1:T(8,128)(2,1)}, u32[]{:S(2)}) copy-start(bf16[1408,64]{0,1:T(8,128)(2,1)} %param.27) | copy-start | bytes 540676
  4.3 16.8 %collective-permute-start.3 = (bf16[64,1536]{1,0:T(8,128)(2,1)S(1)}, bf16[64,1536]{1,0:T(8,128)(2,1)S(1)}, u32[]{:S(2)}, u32[]{:S(2)}) collective-permute-start(bf16[64,1536]{1,0:T(8,128)(2,1)S(1)} %pad_maximum_fusion.3), channel_id=1, source_target_pairs={{0,32},{32,64},{64,96},{96,0},{1,33},{33,65},{65,97},{97,1},{2,34}... | collective-permute-start | bytes 589832 | tf_op jit(solution)/shard_map/ppermute | solution.py:32
  6.1 17.9 %collective-permute-start.4 = (bf16[64,1536]{1,0:T(8,128)(2,1)S(1)}, bf16[64,1536]{1,0:T(8,128)(2,1)S(1)}, u32[]{:S(2)}, u32[]{:S(2)}) collective-permute-start(bf16[64,1536]{1,0:T(8,128)(2,1)S(1)} %pad_maximum_fusion.2.refs_0_), channel_id=1, source_target_pairs={{0,6},{1,25},{2,0},{3,27},{4,2},{5,29},{6,4},{7,31},{8,14},{9,1},{... | collective-permute-start | bytes 589832 | tf_op jit(solution)/shard_map/ppermute | solution.py:64
  8.9 15.4 %collective-permute-start.6 = (bf16[64,1536]{1,0:T(8,128)(2,1)S(1)}, bf16[64,1536]{1,0:T(8,128)(2,1)S(1)}, u32[]{:S(2)}, u32[]{:S(2)}) collective-permute-start(bf16[64,1536]{1,0:T(8,128)(2,1)S(1)} %pad_maximum_fusion.2.refs_0_), channel_id=1, source_target_pairs={{0,4},{1,17},{2,6},{3,19},{4,0},{5,21},{6,2},{7,23},{8,12},{9,25},... | collective-permute-start | bytes 589832 | tf_op jit(solution)/shard_map/ppermute | solution.py:64
  9.2 18.7 %collective-permute-start.8 = (bf16[64,1536]{1,0:T(8,128)(2,1)S(1)}, bf16[64,1536]{1,0:T(8,128)(2,1)S(1)}, u32[]{:S(2)}, u32[]{:S(2)}) collective-permute-start(bf16[64,1536]{1,0:T(8,128)(2,1)S(1)} %pad_maximum_fusion.2.refs_0_), channel_id=1, source_target_pairs={{0,2},{1,9},{2,4},{3,11},{4,6},{5,13},{6,0},{7,15},{8,10},{9,17},{... | collective-permute-start | bytes 589832 | tf_op jit(solution)/shard_map/ppermute | solution.py:64
  21.2 7.5 %collective-permute-start.5 = (bf16[64,1536]{1,0:T(8,128)(2,1)S(1)}, bf16[64,1536]{1,0:T(8,128)(2,1)S(1)}, u32[]{:S(2)}, u32[]{:S(2)}) collective-permute-start(bf16[64,1536]{1,0:T(8,128)(2,1)S(1)} %collective-permute-done.3.refs_1_), channel_id=1, source_target_pairs={{0,6},{1,25},{2,0},{3,27},{4,2},{5,29},{6,4},{7,31},{8,14},{9,1},{... | collective-permute-start | bytes 589832 | tf_op jit(solution)/shard_map/ppermute | solution.py:64
  23.9 6.1 %collective-permute-start.7 = (bf16[64,1536]{1,0:T(8,128)(2,1)S(1)}, bf16[64,1536]{1,0:T(8,128)(2,1)S(1)}, u32[]{:S(2)}, u32[]{:S(2)}) collective-permute-start(bf16[64,1536]{1,0:T(8,128)(2,1)S(1)} %collective-permute-done.3.refs_1_), channel_id=1, source_target_pairs={{0,4},{1,17},{2,6},{3,19},{4,0},{5,21},{6,2},{7,23},{8,12},{9,25},... | collective-permute-start | bytes 589832 | tf_op jit(solution)/shard_map/ppermute | solution.py:64
  24.3 7.8 %collective-permute-start.9 = (bf16[64,1536]{1,0:T(8,128)(2,1)S(1)}, bf16[64,1536]{1,0:T(8,128)(2,1)S(1)}, u32[]{:S(2)}, u32[]{:S(2)}) collective-permute-start(bf16[64,1536]{1,0:T(8,128)(2,1)S(1)} %collective-permute-done.3.refs_1_), channel_id=1, source_target_pairs={{0,2},{1,9},{2,4},{3,11},{4,6},{5,13},{6,0},{7,15},{8,10},{9,17},{... | collective-permute-start | bytes 589832 | tf_op jit(solution)/shard_map/ppermute | solution.py:64
  28.0 25.9 %collective-permute-start = (bf16[256,2048]{1,0:T(8,128)(2,1)S(1)}, bf16[256,2048]{1,0:T(8,128)(2,1)}, u32[]{:S(2)}, u32[]{:S(2)}) collective-permute-start(bf16[256,2048]{1,0:T(8,128)(2,1)S(1)} %shard_map.136.own), channel_id=1, source_target_pairs={{0,1},{1,0},{2,3},{3,2},{4,5},{5,4},{6,7},{7,6},{8,9},{9,8},{10,11... | collective-permute-start | bytes 3145736 | tf_op jit(solution)/shard_map/ppermute | solution.py:36
  34.3 9.7 %collective-permute-start.14 = (bf16[512,512]{1,0:T(8,128)(2,1)}, bf16[512,512]{1,0:T(8,128)(2,1)}, u32[]{:S(2)}, u32[]{:S(2)}) collective-permute-start(bf16[512,512]{1,0:T(8,128)(2,1)} %get-tuple-element.27.rest_0_), channel_id=1, source_target_pairs={{0,8},{1,3},{2,10},{3,5},{4,12},{5,7},{6,14},{7,1},{8,16},{9,11},{... | collective-permute-start | bytes 1572872 | tf_op jit(solution)/shard_map/ppermute | solution.py:64
  36.6 17.2 %collective-permute-start.2 = (bf16[256,2048]{1,0:T(8,128)(2,1)S(1)}, bf16[256,2048]{1,0:T(8,128)(2,1)}, u32[]{:S(2)}, u32[]{:S(2)}) collective-permute-start(bf16[256,2048]{1,0:T(8,128)(2,1)S(1)} %shard_map.137.rem), channel_id=1, source_target_pairs={{0,1},{1,0},{2,3},{3,2},{4,5},{5,4},{6,7},{7,6},{8,9},{9,8},{10,11... | collective-permute-start | bytes 3145736 | tf_op jit(solution)/shard_map/ppermute | solution.py:36
  36.7 8.7 %collective-permute-start.13 = (bf16[512,512]{1,0:T(8,128)(2,1)}, bf16[512,512]{1,0:T(8,128)(2,1)}, u32[]{:S(2)}, u32[]{:S(2)}) collective-permute-start(bf16[512,512]{1,0:T(8,128)(2,1)} %get-tuple-element.27.rest_0_), channel_id=1, source_target_pairs={{0,24},{1,7},{2,26},{3,1},{4,28},{5,3},{6,30},{7,5},{8,0},{9,15},{... | collective-permute-start | bytes 1572872 | tf_op jit(solution)/shard_map/ppermute | solution.py:64
  38.3 12.7 %collective-permute-start.10 = (bf16[512,512]{1,0:T(8,128)(2,1)}, bf16[512,512]{1,0:T(8,128)(2,1)}, u32[]{:S(2)}, u32[]{:S(2)}) collective-permute-start(bf16[512,512]{1,0:T(8,128)(2,1)} %get-tuple-element.26.rest_0_), channel_id=1, source_target_pairs={{0,24},{1,7},{2,26},{3,1},{4,28},{5,3},{6,30},{7,5},{8,0},{9,15},{... | collective-permute-start | bytes 1572872 | tf_op jit(solution)/shard_map/ppermute | solution.py:64
  44.0 9.8 %collective-permute-start.15 = (bf16[512,512]{1,0:T(8,128)(2,1)}, bf16[512,512]{1,0:T(8,128)(2,1)}, u32[]{:S(2)}, u32[]{:S(2)}) collective-permute-start(bf16[512,512]{1,0:T(8,128)(2,1)} %collective-permute-done.14.rest_3_), channel_id=1, source_target_pairs={{0,8},{1,3},{2,10},{3,5},{4,12},{5,7},{6,14},{7,1},{8,16},{9,11},{... | collective-permute-start | bytes 1572872 | tf_op jit(solution)/shard_map/ppermute | solution.py:64
  45.4 19.1 %collective-permute-start.12 = (bf16[512,512]{1,0:T(8,128)(2,1)}, bf16[512,512]{1,0:T(8,128)(2,1)S(1)}, u32[]{:S(2)}, u32[]{:S(2)}) collective-permute-start(bf16[512,512]{1,0:T(8,128)(2,1)} %get-tuple-element.26.rest_0_), channel_id=1, source_target_pairs={{0,8},{1,3},{2,10},{3,5},{4,12},{5,7},{6,14},{7,1},{8,16},{9,11},{... | collective-permute-start | bytes 1572872 | tf_op jit(solution)/shard_map/ppermute | solution.py:64
  51.0 13.6 %collective-permute-start.11 = (bf16[512,512]{1,0:T(8,128)(2,1)}, bf16[512,512]{1,0:T(8,128)(2,1)S(1)}, u32[]{:S(2)}, u32[]{:S(2)}) collective-permute-start(bf16[512,512]{1,0:T(8,128)(2,1)} %collective-permute-done.10.rest_1_), channel_id=1, source_target_pairs={{0,24},{1,7},{2,26},{3,1},{4,28},{5,3},{6,30},{7,5},{8,0},{9,15},{... | collective-permute-start | bytes 1572872 | tf_op jit(solution)/shard_map/ppermute | solution.py:64
  59.2 3.4 %collective-permute-start.16 = (f32[4,4,128]{2,1,0:T(4,128)S(1)}, f32[4,4,128]{2,1,0:T(4,128)S(1)}, u32[]{:S(2)}, u32[]{:S(2)}) collective-permute-start(f32[4,4,128]{2,1,0:T(4,128)S(1)} %get-tuple-element.29), channel_id=1, source_target_pairs={{0,1},{1,0},{2,3},{3,2},{4,5},{5,4},{6,7},{7,6},{8,9},{9,8},{10,11... | collective-permute-start | bytes 24584 | tf_op jit(solution)/shard_map/ppermute | solution.py:36
  59.6 21.6 %collective-permute-start.26 = (bf16[64,2304]{1,0:T(8,128)(2,1)S(1)}, bf16[64,2304]{1,0:T(8,128)(2,1)S(1)}, u32[]{:S(2)}, u32[]{:S(2)}) collective-permute-start(bf16[64,2304]{1,0:T(8,128)(2,1)S(1)} %pad_maximum_fusion.1), channel_id=1, source_target_pairs={{0,96},{32,0},{64,32},{96,64},{1,97},{33,1},{65,33},{97,65},{2,98}... | collective-permute-start | bytes 884744 | tf_op jit(solution)/shard_map/ppermute | solution.py:32
  61.5 12.5 %collective-permute-start.19 = (bf16[512,512]{1,0:T(8,128)(2,1)S(1)}, bf16[512,512]{1,0:T(8,128)(2,1)S(1)}, u32[]{:S(2)}, u32[]{:S(2)}) collective-permute-start(bf16[512,512]{1,0:T(8,128)(2,1)S(1)} %copy-done.4), channel_id=1, source_target_pairs={{0,24},{1,7},{2,26},{3,1},{4,28},{5,3},{6,30},{7,5},{8,0},{9,15},{... | collective-permute-start | bytes 1572872 | tf_op jit(solution)/shard_map/ppermute | solution.py:64
  62.6 11.3 %collective-permute-start.20 = (bf16[512,512]{1,0:T(8,128)(2,1)S(1)}, bf16[512,512]{1,0:T(8,128)(2,1)S(1)}, u32[]{:S(2)}, u32[]{:S(2)}) collective-permute-start(bf16[512,512]{1,0:T(8,128)(2,1)S(1)} %copy-done.4), channel_id=1, source_target_pairs={{0,16},{1,5},{2,18},{3,7},{4,20},{5,1},{6,22},{7,3},{8,24},{9,13},... | collective-permute-start | bytes 1572872 | tf_op jit(solution)/shard_map/ppermute | solution.py:64
  64.5 13.5 %collective-permute-start.21 = (bf16[512,512]{1,0:T(8,128)(2,1)S(1)}, bf16[512,512]{1,0:T(8,128)(2,1)S(1)}, u32[]{:S(2)}, u32[]{:S(2)}) collective-permute-start(bf16[512,512]{1,0:T(8,128)(2,1)S(1)} %copy-done.4), channel_id=1, source_target_pairs={{0,8},{1,3},{2,10},{3,5},{4,12},{5,7},{6,14},{7,1},{8,16},{9,11},{... | collective-permute-start | bytes 1572872 | tf_op jit(solution)/shard_map/ppermute | solution.py:64
  64.6 5.3 %collective-permute-start.18 = (f32[2,4,128]{2,1,0:T(4,128)S(1)}, f32[2,4,128]{2,1,0:T(4,128)S(1)}, u32[]{:S(2)}, u32[]{:S(2)}) collective-permute-start(f32[2,4,128]{2,1,0:T(4,128)S(1)} %pad_maximum_fusion.4), channel_id=1, source_target_pairs={{0,96},{32,0},{64,32},{96,64},{1,97},{33,1},{65,33},{97,65},{2,98}... | collective-permute-start | bytes 12296 | tf_op jit(solution)/shard_map/ppermute | solution.py:32
  69.9 4.0 %collective-permute-start.17 = (f32[2,4,128]{2,1,0:T(4,128)S(1)}, f32[2,4,128]{2,1,0:T(4,128)S(1)}, u32[]{:S(2)}, u32[]{:S(2)}) collective-permute-start(f32[2,4,128]{2,1,0:T(4,128)S(1)} %slice.28), channel_id=1, source_target_pairs={{0,32},{32,64},{64,96},{96,0},{1,33},{33,65},{65,97},{97,1},{2,34}... | collective-permute-start | bytes 12296 | tf_op jit(solution)/shard_map/ppermute | solution.py:32
  80.6 18.1 %collective-permute-start.22 = (bf16[256,2048]{1,0:T(8,128)(2,1)S(1)}, bf16[256,2048]{1,0:T(8,128)(2,1)S(1)}, u32[]{:S(2)}, u32[]{:S(2)}) collective-permute-start(bf16[256,2048]{1,0:T(8,128)(2,1)S(1)} %get-tuple-element.32), channel_id=1, source_target_pairs={{0,1},{1,0},{2,3},{3,2},{4,5},{5,4},{6,7},{7,6},{8,9},{9,8},{10,11... | collective-permute-start | bytes 3145736 | tf_op jit(solution)/shard_map/ppermute | solution.py:36
  81.1 7.1 %collective-permute-start.29 = (bf16[64,2304]{1,0:T(8,128)(2,1)S(1)}, bf16[64,2304]{1,0:T(8,128)(2,1)S(1)}, u32[]{:S(2)}, u32[]{:S(2)}) collective-permute-start(bf16[64,2304]{1,0:T(8,128)(2,1)S(1)} %pad_maximum_fusion.refs_0_), channel_id=1, source_target_pairs={{0,2},{1,9},{2,4},{3,11},{4,6},{5,13},{6,0},{7,15},{8,10},{9,17},{... | collective-permute-start | bytes 884744 | tf_op jit(solution)/shard_map/ppermute | solution.py:64
  81.3 7.0 %collective-permute-start.28 = (bf16[64,2304]{1,0:T(8,128)(2,1)S(1)}, bf16[64,2304]{1,0:T(8,128)(2,1)S(1)}, u32[]{:S(2)}, u32[]{:S(2)}) collective-permute-start(bf16[64,2304]{1,0:T(8,128)(2,1)S(1)} %collective-permute-done.26.refs_1_), channel_id=1, source_target_pairs={{0,6},{1,25},{2,0},{3,27},{4,2},{5,29},{6,4},{7,31},{8,14},{9,1},{... | collective-permute-start | bytes 884744 | tf_op jit(solution)/shard_map/ppermute | solution.py:64
  83.8 9.5 %collective-permute-start.27 = (bf16[64,2304]{1,0:T(8,128)(2,1)S(1)}, bf16[64,2304]{1,0:T(8,128)(2,1)S(1)}, u32[]{:S(2)}, u32[]{:S(2)}) collective-permute-start(bf16[64,2304]{1,0:T(8,128)(2,1)S(1)} %pad_maximum_fusion.refs_0_), channel_id=1, source_target_pairs={{0,6},{1,25},{2,0},{3,27},{4,2},{5,29},{6,4},{7,31},{8,14},{9,1},{... | collective-permute-start | bytes 884744 | tf_op jit(solution)/shard_map/ppermute | solution.py:64
  83.8 11.5 %collective-permute-start.32 = (bf16[64,2304]{1,0:T(8,128)(2,1)S(1)}, bf16[64,2304]{1,0:T(8,128)(2,1)S(1)}, u32[]{:S(2)}, u32[]{:S(2)}) collective-permute-start(bf16[64,2304]{1,0:T(8,128)(2,1)S(1)} %collective-permute-done.26.refs_1_), channel_id=1, source_target_pairs={{0,2},{1,9},{2,4},{3,11},{4,6},{5,13},{6,0},{7,15},{8,10},{9,17},{... | collective-permute-start | bytes 884744 | tf_op jit(solution)/shard_map/ppermute | solution.py:64
  88.2 7.1 %collective-permute-start.30 = (bf16[64,2304]{1,0:T(8,128)(2,1)S(1)}, bf16[64,2304]{1,0:T(8,128)(2,1)S(1)}, u32[]{:S(2)}, u32[]{:S(2)}) collective-permute-start(bf16[64,2304]{1,0:T(8,128)(2,1)S(1)} %collective-permute-done.29.refs_6_), channel_id=1, source_target_pairs={{0,2},{1,9},{2,4},{3,11},{4,6},{5,13},{6,0},{7,15},{8,10},{9,17},{... | collective-permute-start | bytes 884744 | tf_op jit(solution)/shard_map/ppermute | solution.py:64
  88.2 7.1 %collective-permute-start.31 = (bf16[64,2304]{1,0:T(8,128)(2,1)S(1)}, bf16[64,2304]{1,0:T(8,128)(2,1)S(1)}, u32[]{:S(2)}, u32[]{:S(2)}) collective-permute-start(bf16[64,2304]{1,0:T(8,128)(2,1)S(1)} %collective-permute-done.28.refs_3_), channel_id=1, source_target_pairs={{0,6},{1,25},{2,0},{3,27},{4,2},{5,29},{6,4},{7,31},{8,14},{9,1},{... | collective-permute-start | bytes 884744 | tf_op jit(solution)/shard_map/ppermute | solution.py:64
  93.4 16.2 %collective-permute-start.23 = (bf16[256,2048]{1,0:T(8,128)(2,1)S(1)}, bf16[256,2048]{1,0:T(8,128)(2,1)S(1)}, u32[]{:S(2)}, u32[]{:S(2)}) collective-permute-start(bf16[256,2048]{1,0:T(8,128)(2,1)S(1)} %get-tuple-element.34), channel_id=1, source_target_pairs={{0,1},{1,0},{2,3},{3,2},{4,5},{5,4},{6,7},{7,6},{8,9},{9,8},{10,11... | collective-permute-start | bytes 3145736 | tf_op jit(solution)/shard_map/ppermute | solution.py:36
  95.9 12.4 %collective-permute-start.34 = (bf16[512,768]{1,0:T(8,128)(2,1)S(1)}, bf16[512,768]{1,0:T(8,128)(2,1)S(1)}, u32[]{:S(2)}, u32[]{:S(2)}) collective-permute-start(bf16[512,768]{1,0:T(8,128)(2,1)S(1)} %get-tuple-element.37.refs_0_), channel_id=1, source_target_pairs={{0,8},{1,3},{2,10},{3,5},{4,12},{5,7},{6,14},{7,1},{8,16},{9,11},{... | collective-permute-start | bytes 2359304 | tf_op jit(solution)/shard_map/ppermute | solution.py:64
  96.3 12.1 %collective-permute-start.36 = (bf16[512,768]{1,0:T(8,128)(2,1)S(1)}, bf16[512,768]{1,0:T(8,128)(2,1)S(1)}, u32[]{:S(2)}, u32[]{:S(2)}) collective-permute-start(bf16[512,768]{1,0:T(8,128)(2,1)S(1)} %get-tuple-element.38.refs_4_), channel_id=1, source_target_pairs={{0,24},{1,7},{2,26},{3,1},{4,28},{5,3},{6,30},{7,5},{8,0},{9,15},{... | collective-permute-start | bytes 2359304 | tf_op jit(solution)/shard_map/ppermute | solution.py:64
  99.0 14.9 %collective-permute-start.43 = (bf16[256,2048]{1,0:T(8,128)(2,1)S(1)}, bf16[256,2048]{1,0:T(8,128)(2,1)S(1)}, u32[]{:S(2)}, u32[]{:S(2)}) collective-permute-start(bf16[256,2048]{1,0:T(8,128)(2,1)S(1)} %shard_map.142.refs_1_), channel_id=1, source_target_pairs={{0,96},{1,33},{32,0},{33,65},{64,32},{65,97},{96,64},{97,1},{2,98}... | collective-permute-start | bytes 3145736 | tf_op jit(solution)/shard_map/ppermute | solution.py:44
  99.2 17.0 %collective-permute-start.33 = (bf16[512,768]{1,0:T(8,128)(2,1)S(1)}, bf16[512,768]{1,0:T(8,128)(2,1)S(1)}, u32[]{:S(2)}, u32[]{:S(2)}) collective-permute-start(bf16[512,768]{1,0:T(8,128)(2,1)S(1)} %get-tuple-element.37.refs_0_), channel_id=1, source_target_pairs={{0,24},{1,7},{2,26},{3,1},{4,28},{5,3},{6,30},{7,5},{8,0},{9,15},{... | collective-permute-start | bytes 2359304 | tf_op jit(solution)/shard_map/ppermute | solution.py:64
  108.4 24.5 %collective-permute-start.39 = (bf16[512,768]{1,0:T(8,128)(2,1)S(1)}, bf16[512,768]{1,0:T(8,128)(2,1)S(1)}, u32[]{:S(2)}, u32[]{:S(2)}) collective-permute-start(bf16[512,768]{1,0:T(8,128)(2,1)S(1)} %get-tuple-element.41.refs_0_), channel_id=1, source_target_pairs={{0,24},{1,7},{2,26},{3,1},{4,28},{5,3},{6,30},{7,5},{8,0},{9,15},{... | collective-permute-start | bytes 2359304 | tf_op jit(solution)/shard_map/ppermute | solution.py:64
  108.4 24.5 %collective-permute-start.40 = (bf16[512,768]{1,0:T(8,128)(2,1)S(1)}, bf16[512,768]{1,0:T(8,128)(2,1)S(1)}, u32[]{:S(2)}, u32[]{:S(2)}) collective-permute-start(bf16[512,768]{1,0:T(8,128)(2,1)S(1)} %get-tuple-element.41.refs_0_), channel_id=1, source_target_pairs={{0,16},{1,5},{2,18},{3,7},{4,20},{5,1},{6,22},{7,3},{8,24},{9,13},... | collective-permute-start | bytes 2359304 | tf_op jit(solution)/shard_map/ppermute | solution.py:64
  109.6 24.4 %collective-permute-start.41 = (bf16[512,768]{1,0:T(8,128)(2,1)S(1)}, bf16[512,768]{1,0:T(8,128)(2,1)S(1)}, u32[]{:S(2)}, u32[]{:S(2)}) collective-permute-start(bf16[512,768]{1,0:T(8,128)(2,1)S(1)} %get-tuple-element.41.refs_0_), channel_id=1, source_target_pairs={{0,8},{1,3},{2,10},{3,5},{4,12},{5,7},{6,14},{7,1},{8,16},{9,11},{... | collective-permute-start | bytes 2359304 | tf_op jit(solution)/shard_map/ppermute | solution.py:64
  113.9 41.0 %collective-permute-start.24 = (bf16[256,2048]{1,0:T(8,128)(2,1)S(1)}, bf16[256,2048]{1,0:T(8,128)(2,1)S(1)}, u32[]{:S(2)}, u32[]{:S(2)}) collective-permute-start(bf16[256,2048]{1,0:T(8,128)(2,1)S(1)} %shard_map.144.refs_1_), channel_id=1, source_target_pairs={{0,32},{1,97},{32,64},{33,1},{64,96},{65,33},{96,0},{97,65},{2,34}... | collective-permute-start | bytes 3145736 | tf_op jit(solution)/shard_map/ppermute | solution.py:52
  116.2 43.8 %collective-permute-start.44 = (bf16[256,2048]{1,0:T(8,128)(2,1)S(1)}, bf16[256,2048]{1,0:T(8,128)(2,1)S(1)}, u32[]{:S(2)}, u32[]{:S(2)}) collective-permute-start(bf16[256,2048]{1,0:T(8,128)(2,1)S(1)} %get-tuple-element.44.first), channel_id=1, source_target_pairs={{0,1},{1,0},{2,3},{3,2},{4,5},{5,4},{6,7},{7,6},{8,9},{9,8},{10,11... | collective-permute-start | bytes 3145736 | tf_op jit(solution)/shard_map/ppermute | solution.py:36
  132.9 13.1 %collective-permute-start.38 = (bf16[512,768]{1,0:T(8,128)(2,1)S(1)}, bf16[512,768]{1,0:T(8,128)(2,1)S(1)}, u32[]{:S(2)}, u32[]{:S(2)}) collective-permute-start(bf16[512,768]{1,0:T(8,128)(2,1)S(1)} %get-tuple-element.38.refs_4_), channel_id=1, source_target_pairs={{0,8},{1,3},{2,10},{3,5},{4,12},{5,7},{6,14},{7,1},{8,16},{9,11},{... | collective-permute-start | bytes 2359304 | tf_op jit(solution)/shard_map/ppermute | solution.py:64
  132.9 21.5 %collective-permute-start.35 = (bf16[512,768]{1,0:T(8,128)(2,1)S(1)}, bf16[512,768]{1,0:T(8,128)(2,1)S(1)}, u32[]{:S(2)}, u32[]{:S(2)}) collective-permute-start(bf16[512,768]{1,0:T(8,128)(2,1)S(1)} %collective-permute-done.34.refs_3_), channel_id=1, source_target_pairs={{0,8},{1,3},{2,10},{3,5},{4,12},{5,7},{6,14},{7,1},{8,16},{9,11},{... | collective-permute-start | bytes 2359304 | tf_op jit(solution)/shard_map/ppermute | solution.py:64
  133.9 20.5 %collective-permute-start.37 = (bf16[512,768]{1,0:T(8,128)(2,1)S(1)}, bf16[512,768]{1,0:T(8,128)(2,1)S(1)}, u32[]{:S(2)}, u32[]{:S(2)}) collective-permute-start(bf16[512,768]{1,0:T(8,128)(2,1)S(1)} %collective-permute-done.36.refs_5_), channel_id=1, source_target_pairs={{0,24},{1,7},{2,26},{3,1},{4,28},{5,3},{6,30},{7,5},{8,0},{9,15},{... | collective-permute-start | bytes 2359304 | tf_op jit(solution)/shard_map/ppermute | solution.py:64
  156.3 9.3 %collective-permute-start.25 = (bf16[256,2048]{1,0:T(8,128)(2,1)S(1)}, bf16[256,2048]{1,0:T(8,128)(2,1)S(1)}, u32[]{:S(2)}, u32[]{:S(2)}) collective-permute-start(bf16[256,2048]{1,0:T(8,128)(2,1)S(1)} %get-tuple-element.36.first), channel_id=1, source_target_pairs={{0,1},{1,0},{2,3},{3,2},{4,5},{5,4},{6,7},{7,6},{8,9},{9,8},{10,11... | collective-permute-start | bytes 3145736 | tf_op jit(solution)/shard_map/ppermute | solution.py:36
  165.5 6.2 %collective-permute-start.45 = (bf16[256,2048]{1,0:T(8,128)(2,1)S(1)}, bf16[256,2048]{1,0:T(8,128)(2,1)S(1)}, u32[]{:S(2)}, u32[]{:S(2)}) collective-permute-start(bf16[256,2048]{1,0:T(8,128)(2,1)S(1)} %get-tuple-element.46), channel_id=1, source_target_pairs={{0,1},{1,0},{2,3},{3,2},{4,5},{5,4},{6,7},{7,6},{8,9},{9,8},{10,11... | collective-permute-start | bytes 3145736 | tf_op jit(solution)/shard_map/ppermute | solution.py:36
  171.2 2.8 %collective-permute-start.42 = (bf16[256,2048]{1,0:T(8,128)(2,1)S(1)}, bf16[256,2048]{1,0:T(8,128)(2,1)S(1)}, u32[]{:S(2)}, u32[]{:S(2)}) collective-permute-start(bf16[256,2048]{1,0:T(8,128)(2,1)S(1)} %get-tuple-element.43), channel_id=1, source_target_pairs={{0,1},{1,0},{2,3},{3,2},{4,5},{5,4},{6,7},{7,6},{8,9},{9,8},{10,11... | collective-permute-start | bytes 3145736 | tf_op jit(solution)/shard_map/ppermute | solution.py:36
  172.1 14.0 %collective-permute-start.46 = (bf16[256,2048]{1,0:T(8,128)(2,1)S(1)}, bf16[256,2048]{1,0:T(8,128)(2,1)S(1)}, u32[]{:S(2)}, u32[]{:S(2)}) collective-permute-start(bf16[256,2048]{1,0:T(8,128)(2,1)S(1)} %shard_map.154), channel_id=1, source_target_pairs={{0,32},{1,97},{32,64},{33,1},{64,96},{65,33},{96,0},{97,65},{2,34}... | collective-permute-start | bytes 3145736 | tf_op jit(solution)/shard_map/ppermute | solution.py:52
  (12 other events, 150.0 us)
where the time goes:
time: 189 us; the launch traced here: 188 us
  waiting for transfers between devices  90.5 us (48%)
  starting transfers between devices  53.8 us (28%)
  Pallas kernels  37.1 us (20%)
  local copies, waits for them, and re-layouts  5.65 us (3%)
    ppermute x30, waiting for transfers between devices, along(): return lax.ppermute(value, YXT, pairs)  61 us
    ppermute x30, starting transfers between devices, along(): return lax.ppermute(value, YXT, pairs)  35.6 us
    pallas_call x8, Pallas kernels, call(): pl.pallas_call(kernel, out_shape=out_shape, in_specs=[VM] * len(args), ou...  26.3 us
    ppermute x4, waiting for transfers between devices, ring(): return lax.ppermute(value, axis, [(i, (i + by) % 4) for i in range(4)])  13.9 us
    ppermute x2, waiting for transfers between devices, to_owner(): return lax.ppermute(value, ZT, pairs)  12 us
    ppermute x9, starting transfers between devices, other_core(): return lax.ppermute(value, 'tp', [(0, 1), (1, 0)])  9.77 us
    pallas_call x6, Pallas kernels, plus(): pl.pallas_call(functools.partial(plus_kernel, len(arrays), gain is not No...  5.96 us
    ppermute x4, starting transfers between devices, ring(): return lax.ppermute(value, axis, [(i, (i + by) % 4) for i in range(4)])  5.32 us
  transfers between devices with their start and end apart: 47, of which 18 were waited for; matrix products, arithmetic and copies ran while one was open for 2% of the time, Pallas kernels for 19%

commit v1 on v0

--- a/solution.py
+++ b/solution.py
@@ -109,7 +109,11 @@
 def plane_second(line, route):
     back = along(line, False, 1)
     ahead = along(line, False, -1)
-    return (line, ahead, furthest(line, ahead, back, False, route), back)
+    if route == 2:
+        far = (along(back[:256], False, 1), along(ahead[256:], False, -1))
+    else:
+        far = (furthest(line, ahead, back, False, route),)
+    return (line, ahead, *far, back)
 
 
 PLACES = [(s, f * 128 + h * 64, f, s, h) for s in range(4) for f in range(4) for h in range(2)]
@@ -124,6 +128,8 @@
         dx = first + t * (second - first)
         dy = second + t * (first - second)
         block = lax.rem(a + half, 2) * 16 + lax.rem(y + dy, 4) * 4 + lax.rem(x + dx, 4)
+        if len(refs) == 5 and (which == 3 or which == 2 and row >= 256):
+            which, row = which + 1, row % 256 if which == 2 else row
         held[pl.ds(pl.multiple_of(block * 64, 64), 64), :] = refs[which][row : row + 64, :]
 
 
@@ -217,10 +223,11 @@
         outs[s][...] = out.astype(BF16)
 
 
-def assemble_kernel(*refs):
-    n = len(refs) // 5
-    for k in range(n):
-        place_weight(refs[4 * k : 4 * k + 4], refs[4 * n + k])
+def assemble_kernel(sizes, *refs):
+    begin = 0
+    for k, size in enumerate(sizes):
+        place_weight(refs[begin : begin + size], refs[sum(sizes) + k])
+        begin += size
 
 
 def hidden_kernel(first, second, wgate, wup, taps_all, hidden):
@@ -330,10 +337,10 @@
     mixer_arrays = (spatial_proj, gating_proj, mixer_out.T)
     channel_arrays = (gate_proj, up_proj, down_proj.T)
 
-    def first_phase(arrays, step, width, by, routes):
+    def first_phase(arrays, step, width, routes):
         give = window(arrays, 1 - a, step, width)
         mine = window(arrays, a, step, width)
-        theirs = ring(give, Z, by)
+        theirs = to_owner(give)
         firsts = zip(plane_first(mine, routes[0]), plane_first(theirs, routes[1]))
         return [piece for both in firsts for piece in both]
 
@@ -343,16 +350,16 @@
     own2_n = other_core(own_n)
     rem_n = normed(rem, mixer_gain[None])
     rem2_n = other_core(rem_n)
-    m_first = first_phase(mixer_arrays, QM, QM, 1, (0, 0))
+    m_first = first_phase(mixer_arrays, QM, QM, (0, 0))
     s_line, u_line, o_line = joined(m_first, (QM,) * 3)
     s_pieces = plane_second(s_line, 1)
     u_pieces = plane_second(u_line, -1)
     o_pieces = plane_second(o_line, 0)
-    c_first = first_phase(channel_arrays, QSTEP, QC, -1, (1, -1))
+    c_first = first_phase(channel_arrays, QSTEP, QC, (1, -1))
     g_line, h_line, d_line = joined(c_first, (QC,) * 3)
     g_pieces = plane_second(g_line, 1)
     h_pieces = plane_second(h_line, -1)
-    d_pieces = plane_second(d_line, 0)
+    d_pieces = plane_second(d_line, 2)
     seqs = (own_n, own2_n, rem_n, rem2_n)
 
     act_v, sums = call(
@@ -400,7 +407,7 @@
     def assembled(*groups):
         flat = [p for g in groups for p in g]
         return pl.pallas_call(
-            assemble_kernel,
+            functools.partial(assemble_kernel, [len(g) for g in groups]),
             out_shape=[arr((D, QC), BF16)] * len(groups),
             in_specs=[VM] * len(flat),
             out_specs=[VM] * len(groups),

time: 189 us -> 182 us (0.963)
  waiting for transfers between devices: 90.5 us -> 79.9 us
  starting transfers between devices: 53.8 us -> 59.7 us
  local copies, waits for them, and re-layouts: 5.65 us -> 3.02 us
    ppermute x4 -> x2, waiting for transfers between devices: 13.9 us -> 1.97 us  [ring(): return lax.ppermute(value, axis, [(i, (i + by) % 4) for i in range(4)])]
    ppermute x9, starting transfers between devices: 9.77 us -> 20.4 us  [other_core(): return lax.ppermute(value, 'tp', [(0, 1), (1, 0)])]
    ppermute x30 -> x31, starting transfers between devices: 35.6 us -> 31.5 us  [along(): return lax.ppermute(value, YXT, pairs)]
    ppermute x4 -> x2, starting transfers between devices: 5.32 us -> 1.53 us  [ring(): return lax.ppermute(value, axis, [(i, (i + by) % 4) for i in range(4)])]
    ppermute x2 -> x4, starting transfers between devices: 0.49 us -> 3.74 us  [to_owner(): return lax.ppermute(value, ZT, pairs)]
    unnamed x26 -> x28, local copies, waits for them, and re-layouts: 2.76 us -> 0.07 us
    ppermute x2, waiting for transfers between devices: 2.01 us -> 0.01 us  [to_partner(): return lax.ppermute(value, ZT, pairs)]
    ppermute x30 -> x31, waiting for transfers between devices: 61 us -> 62.3 us  [along(): return lax.ppermute(value, YXT, pairs)]
  transfers between devices with their start and end apart: 47 -> 48, of which waited for: 18 -> 19; matrix products, arithmetic and copies ran while one was open for 2% -> 2% of each run, Pallas kernels for 19% -> 20%
where the time goes in v1:
time: 182 us; the launch traced here: 181 us
  waiting for transfers between devices  79.9 us (44%)
  starting transfers between devices  59.7 us (33%)
  Pallas kernels  37.9 us (21%)
  local copies, waits for them, and re-layouts  3.02 us (2%)
    ppermute x31, waiting for transfers between devices, along(): return lax.ppermute(value, YXT, pairs)  62.3 us
    ppermute x31, starting transfers between devices, along(): return lax.ppermute(value, YXT, pairs)  31.5 us
    pallas_call x8, Pallas kernels, call(): pl.pallas_call(kernel, out_shape=out_shape, in_specs=[VM] * len(args), ou...  26.3 us
    ppermute x9, starting transfers between devices, other_core(): return lax.ppermute(value, 'tp', [(0, 1), (1, 0)])  20.4 us
    ppermute x4, waiting for transfers between devices, to_owner(): return lax.ppermute(value, ZT, pairs)  13 us
    pallas_call x6, Pallas kernels, plus(): pl.pallas_call(functools.partial(plus_kernel, len(arrays), gain is not No...  5.96 us
    ppermute x4, starting transfers between devices, to_owner(): return lax.ppermute(value, ZT, pairs)  3.74 us
  transfers between devices with their start and end apart: 48, of which 19 were waited for; matrix products, arithmetic and copies ran while one was open for 2% of the time, Pallas kernels for 20%

profile of v1, /device:TPU:1, one launch (start us, length us, event | category | flops | bytes accessed | tf_op | source)
XLA Modules:
  0.0 181.0 jit_solution(8876965216063693602)
XLA Ops:
  0.0 2.5 %collective-permute-start.1 = (bf16[256,2048]{1,0:T(8,128)(2,1)}, bf16[256,2048]{1,0:T(8,128)(2,1)S(1)}, u32[]{:S(2)}, u32[]{:S(2)}) collective-permute-start(bf16[256,2048]{1,0:T(8,128)(2,1)} %refs_0_.1), channel_id=1, source_target_pairs={{0,96},{1,33},{32,0},{33,65},{64,32},{65,97},{96,64},{97,1},{2,98}... | collective-permute-start | bytes 3145736 | tf_op jit(solution)/shard_map/ppermute | solution.py:44
  4.3 2.3 %collective-permute-start.3 = (bf16[64,1536]{1,0:T(8,128)(2,1)S(1)}, bf16[64,1536]{1,0:T(8,128)(2,1)S(1)}, u32[]{:S(2)}, u32[]{:S(2)}) collective-permute-start(bf16[64,1536]{1,0:T(8,128)(2,1)S(1)} %pad_maximum_fusion.3), channel_id=1, source_target_pairs={{0,32},{1,97},{32,64},{33,1},{64,96},{65,33},{96,0},{97,65},{2,34}... | collective-permute-start | bytes 589832 | tf_op jit(solution)/shard_map/ppermute | solution.py:52
  6.7 2.8 %collective-permute-start.4 = (bf16[64,1536]{1,0:T(8,128)(2,1)S(1)}, bf16[64,1536]{1,0:T(8,128)(2,1)S(1)}, u32[]{:S(2)}, u32[]{:S(2)}) collective-permute-start(bf16[64,1536]{1,0:T(8,128)(2,1)S(1)} %pad_maximum_fusion.2.refs_0_), channel_id=1, source_target_pairs={{0,6},{1,25},{2,0},{3,27},{4,2},{5,29},{6,4},{7,31},{8,14},{9,1},{... | collective-permute-start | bytes 589832 | tf_op jit(solution)/shard_map/ppermute | solution.py:64
  11.5 2.7 %collective-permute-start.5 = (bf16[64,1536]{1,0:T(8,128)(2,1)S(1)}, bf16[64,1536]{1,0:T(8,128)(2,1)S(1)}, u32[]{:S(2)}, u32[]{:S(2)}) collective-permute-start(bf16[64,1536]{1,0:T(8,128)(2,1)S(1)} %collective-permute-done.3.refs_1_), channel_id=1, source_target_pairs={{0,6},{1,25},{2,0},{3,27},{4,2},{5,29},{6,4},{7,31},{8,14},{9,1},{... | collective-permute-start | bytes 589832 | tf_op jit(solution)/shard_map/ppermute | solution.py:64
  15.8 2.4 %collective-permute-start.9 = (bf16[64,1536]{1,0:T(8,128)(2,1)S(1)}, bf16[64,1536]{1,0:T(8,128)(2,1)S(1)}, u32[]{:S(2)}, u32[]{:S(2)}) collective-permute-start(bf16[64,1536]{1,0:T(8,128)(2,1)S(1)} %collective-permute-done.3.refs_1_), channel_id=1, source_target_pairs={{0,2},{1,9},{2,4},{3,11},{4,6},{5,13},{6,0},{7,15},{8,10},{9,17},{... | collective-permute-start | bytes 589832 | tf_op jit(solution)/shard_map/ppermute | solution.py:64
  18.2 2.2 %collective-permute-done.7.refs_5_ = bf16[64,1536]{1,0:T(8,128)(2,1)S(1)} collective-permute-done((bf16[64,1536]{1,0:T(8,128)(2,1)S(1)}, bf16[64,1536]{1,0:T(8,128)(2,1)S(1)}, u32[]{:S(2)}, u32[]{:S(2)}) %collective-permute-start.7) | collective-permute-done | bytes 196640 | tf_op jit(solution)/shard_map/ppermute | solution.py:64
  20.4 2.0 %collective-permute-done.9.refs_7_ = bf16[64,1536]{1,0:T(8,128)(2,1)S(1)} collective-permute-done((bf16[64,1536]{1,0:T(8,128)(2,1)S(1)}, bf16[64,1536]{1,0:T(8,128)(2,1)S(1)}, u32[]{:S(2)}, u32[]{:S(2)}) %collective-permute-start.9) | collective-permute-done | bytes 196640 | tf_op jit(solution)/shard_map/ppermute | solution.py:64
  22.4 1.3 shard_map.138
  26.0 7.5 %collective-permute-start = (bf16[256,2048]{1,0:T(8,128)(2,1)S(1)}, bf16[256,2048]{1,0:T(8,128)(2,1)}, u32[]{:S(2)}, u32[]{:S(2)}) collective-permute-start(bf16[256,2048]{1,0:T(8,128)(2,1)S(1)} %shard_map.136.own), channel_id=1, source_target_pairs={{0,1},{1,0},{2,3},{3,2},{4,5},{5,4},{6,7},{7,6},{8,9},{9,8},{10,11... | collective-permute-start | bytes 3145736 | tf_op jit(solution)/shard_map/ppermute | solution.py:36
  33.5 2.0 %shard_map.137.rem = bf16[256,2048]{1,0:T(8,128)(2,1)} custom-call(bf16[256,2048]{1,0:T(8,128)(2,1)S(1)} %collective-permute-done.1.rows_in.refs_0_, f32[1,2048]{1,0:T(1,128)S(1)} %bitcast.13), custom_call_target="tpu_custom_call" | custom-call | flops 1048576 | bytes 2097152 | tf_op jit(solution)/shard_map/pallas_call | solution.py:300
  35.6 1.5 collective-permute-start.15
  38.2 6.0 %collective-permute-done.13.rest_1_ = bf16[512,512]{1,0:T(8,128)(2,1)S(1)} collective-permute-done((bf16[512,512]{1,0:T(8,128)(2,1)}, bf16[512,512]{1,0:T(8,128)(2,1)S(1)}, u32[]{:S(2)}, u32[]{:S(2)}) %collective-permute-start.13) | collective-permute-done | bytes 524320 | tf_op jit(solution)/shard_map/ppermute | solution.py:64
  44.1 5.6 %collective-permute-done.10.rest_1_ = bf16[512,512]{1,0:T(8,128)(2,1)S(1)} collective-permute-done((bf16[512,512]{1,0:T(8,128)(2,1)}, bf16[512,512]{1,0:T(8,128)(2,1)S(1)}, u32[]{:S(2)}, u32[]{:S(2)}) %collective-permute-start.10) | collective-permute-done | bytes 524320 | tf_op jit(solution)/shard_map/ppermute | solution.py:64
  49.8 2.7 %collective-permute-start.11 = (bf16[512,512]{1,0:T(8,128)(2,1)S(1)}, bf16[512,512]{1,0:T(8,128)(2,1)S(1)}, u32[]{:S(2)}, u32[]{:S(2)}) collective-permute-start(bf16[512,512]{1,0:T(8,128)(2,1)S(1)} %collective-permute-done.10.rest_1_), channel_id=1, source_target_pairs={{0,24},{1,7},{2,26},{3,1},{4,28},{5,3},{6,30},{7,5},{8,0},{9,15},{... | collective-permute-start | bytes 1572872 | tf_op jit(solution)/shard_map/ppermute | solution.py:64
  52.4 5.4 %shard_map.140 = (f32[1024,512]{1,0:T(8,128)S(1)}, f32[4,4,128]{2,1,0:T(4,128)S(1)}) custom-call(bf16[256,2048]{1,0:T(8,128)(2,1)S(1)} %shard_map.136.own, bf16[256,2048]{1,0:T(8,128)(2,1)} %collective-permute-done.own2, bf16[256,2048]{1,0:T(8,128)(2,1)} %shard_map.137.rem, bf16[256,2048]{1,0:T(8,128)(2,1)} %collective-permute-done.2.rem2, ...), custom_call_target="tpu_custom_call" | custom-call | flops 2147483648 | bytes 8388608 | tf_op jit(solution)/shard_map/pallas_call | solution.py:260
  57.8 2.6 %collective-permute-start.16 = (f32[4,4,128]{2,1,0:T(4,128)S(1)}, f32[4,4,128]{2,1,0:T(4,128)S(1)}, u32[]{:S(2)}, u32[]{:S(2)}) collective-permute-start(f32[4,4,128]{2,1,0:T(4,128)S(1)} %get-tuple-element.29), channel_id=1, source_target_pairs={{0,1},{1,0},{2,3},{3,2},{4,5},{5,4},{6,7},{7,6},{8,9},{9,8},{10,11... | collective-permute-start | bytes 24584 | tf_op jit(solution)/shard_map/ppermute | solution.py:36
  62.2 4.9 %shard_map.139.act_u = f32[1024,512]{1,0:T(8,128)S(1)} custom-call(bf16[256,2048]{1,0:T(8,128)(2,1)S(1)} %shard_map.136.own, bf16[256,2048]{1,0:T(8,128)(2,1)} %collective-permute-done.own2, bf16[256,2048]{1,0:T(8,128)(2,1)} %shard_map.137.rem, bf16[256,2048]{1,0:T(8,128)(2,1)} %collective-permute-done.2.rem2, bf16[512,512]{1,0:T(8,128)(2,1)S(1)} %copy-done.5, ...), custom_call_target="tpu_custom_call" | custom-call | flops 2147483648 | bytes 8388608 | tf_op jit(solution)/shard_map/pallas_call | solution.py:260
  67.1 1.5 collective-permute-start.17
  69.2 2.0 %collective-permute-done.17 = f32[2,4,128]{2,1,0:T(4,128)S(1)} collective-permute-done((f32[2,4,128]{2,1,0:T(4,128)S(1)}, f32[2,4,128]{2,1,0:T(4,128)S(1)}, u32[]{:S(2)}, u32[]{:S(2)}) %collective-permute-start.17) | collective-permute-done | bytes 4128 | tf_op jit(solution)/shard_map/ppermute | solution.py:32
  71.1 1.3 collective-permute-start.28
  72.5 5.4 %collective-permute-done.21.rest_3_ = bf16[512,512]{1,0:T(8,128)(2,1)S(1)} collective-permute-done((bf16[512,512]{1,0:T(8,128)(2,1)S(1)}, bf16[512,512]{1,0:T(8,128)(2,1)S(1)}, u32[]{:S(2)}, u32[]{:S(2)}) %collective-permute-start.21) | collective-permute-done | bytes 524320 | tf_op jit(solution)/shard_map/ppermute | solution.py:64
  77.9 2.5 %shard_map.141 = (bf16[256,2048]{1,0:T(8,128)(2,1)S(1)}, bf16[256,2048]{1,0:T(8,128)(2,1)S(1)}) custom-call(f32[1024,512]{1,0:T(8,128)S(1)} %shard_map.139.act_u, f32[1024,512]{1,0:T(8,128)S(1)} %get-tuple-element.28.act_v, f32[4,4,128]{2,1,0:T(4,128)S(1)} %maximum_add_fusion.sums, f32[1,2048]{1,0:T(1,128)S(1)} %bitcast.16, f32[1,2048]{1,0:T(1,128)S(1)} %bitcast.18, ...), custom_call_target="tpu_custom_call" | custom-call | flops 1073741824 | bytes 8388608 | tf_op jit(solution)/shard_map/pallas_call | solution.py:260
  80.3 3.9 %collective-permute-start.22 = (bf16[256,2048]{1,0:T(8,128)(2,1)S(1)}, bf16[256,2048]{1,0:T(8,128)(2,1)S(1)}, u32[]{:S(2)}, u32[]{:S(2)}) collective-permute-start(bf16[256,2048]{1,0:T(8,128)(2,1)S(1)} %get-tuple-element.32), channel_id=1, source_target_pairs={{0,1},{1,0},{2,3},{3,2},{4,5},{5,4},{6,7},{7,6},{8,9},{9,8},{10,11... | collective-permute-start | bytes 3145736 | tf_op jit(solution)/shard_map/ppermute | solution.py:36
  85.7 2.7 %collective-permute-start.31 = (bf16[64,2304]{1,0:T(8,128)(2,1)S(1)}, bf16[64,2304]{1,0:T(8,128)(2,1)S(1)}, u32[]{:S(2)}, u32[]{:S(2)}) collective-permute-start(bf16[64,2304]{1,0:T(8,128)(2,1)S(1)} %collective-permute-done.28.refs_3_), channel_id=1, source_target_pairs={{0,6},{1,25},{2,0},{3,27},{4,2},{5,29},{6,4},{7,31},{8,14},{9,1},{... | collective-permute-start | bytes 884744 | tf_op jit(solution)/shard_map/ppermute | solution.py:64
  88.4 1.7 collective-permute-done.27.refs_2_
  90.1 4.7 %collective-permute-done.30.refs_4_ = bf16[64,2304]{1,0:T(8,128)(2,1)S(1)} collective-permute-done((bf16[64,2304]{1,0:T(8,128)(2,1)S(1)}, bf16[64,2304]{1,0:T(8,128)(2,1)S(1)}, u32[]{:S(2)}, u32[]{:S(2)}) %collective-permute-start.30) | collective-permute-done | bytes 294944 | tf_op jit(solution)/shard_map/ppermute | solution.py:64
  95.5 2.7 %collective-permute-start.39 = (bf16[512,768]{1,0:T(8,128)(2,1)S(1)}, bf16[512,768]{1,0:T(8,128)(2,1)S(1)}, u32[]{:S(2)}, u32[]{:S(2)}) collective-permute-start(bf16[512,768]{1,0:T(8,128)(2,1)S(1)} %get-tuple-element.41.refs_0_), channel_id=1, source_target_pairs={{0,24},{1,7},{2,26},{3,1},{4,28},{5,3},{6,30},{7,5},{8,0},{9,15},{... | collective-permute-start | bytes 2359304 | tf_op jit(solution)/shard_map/ppermute | solution.py:64
  98.2 2.5 %shard_map.143 = (bf16[256,2048]{1,0:T(8,128)(2,1)S(1)}, bf16[256,2048]{1,0:T(8,128)(2,1)S(1)}) custom-call(f32[1024,512]{1,0:T(8,128)S(1)} %shard_map.139.act_u, f32[1024,512]{1,0:T(8,128)S(1)} %get-tuple-element.28.act_v, f32[4,4,128]{2,1,0:T(4,128)S(1)} %maximum_add_fusion.sums, f32[1,2048]{1,0:T(1,128)S(1)} %bitcast.17, f32[1,2048]{1,0:T(1,128)S(1)} %bitcast.19, ...), custom_call_target="tpu_custom_call" | custom-call | flops 1073741824 | bytes 8388608 | tf_op jit(solution)/shard_map/pallas_call | solution.py:260
  100.6 1.3 collective-permute-start.23
  102.9 5.0 %collective-permute-done.40.refs_4_ = bf16[512,768]{1,0:T(8,128)(2,1)S(1)} collective-permute-done((bf16[512,768]{1,0:T(8,128)(2,1)S(1)}, bf16[512,768]{1,0:T(8,128)(2,1)S(1)}, u32[]{:S(2)}, u32[]{:S(2)}) %collective-permute-start.40) | collective-permute-done | bytes 786464 | tf_op jit(solution)/shard_map/ppermute | solution.py:64
  107.8 2.7 %collective-permute-start.33 = (bf16[512,768]{1,0:T(8,128)(2,1)S(1)}, bf16[512,768]{1,0:T(8,128)(2,1)S(1)}, u32[]{:S(2)}, u32[]{:S(2)}) collective-permute-start(bf16[512,768]{1,0:T(8,128)(2,1)S(1)} %get-tuple-element.37.refs_0_), channel_id=1, source_target_pairs={{0,24},{1,7},{2,26},{3,1},{4,28},{5,3},{6,30},{7,5},{8,0},{9,15},{... | collective-permute-start | bytes 2359304 | tf_op jit(solution)/shard_map/ppermute | solution.py:64
  110.6 5.7 %collective-permute-done.34.refs_3_ = bf16[512,768]{1,0:T(8,128)(2,1)S(1)} collective-permute-done((bf16[512,768]{1,0:T(8,128)(2,1)S(1)}, bf16[512,768]{1,0:T(8,128)(2,1)S(1)}, u32[]{:S(2)}, u32[]{:S(2)}) %collective-permute-start.34) | collective-permute-done | bytes 786464 | tf_op jit(solution)/shard_map/ppermute | solution.py:64
  116.3 2.7 %collective-permute-start.42 = (bf16[256,768]{1,0:T(8,128)(2,1)S(1)}, bf16[256,768]{1,0:T(8,128)(2,1)S(1)}, u32[]{:S(2)}, u32[]{:S(2)}) collective-permute-start(bf16[256,768]{1,0:T(8,128)(2,1)S(1)} %slice.44), channel_id=1, source_target_pairs={{0,24},{1,7},{2,26},{3,1},{4,28},{5,3},{6,30},{7,5},{8,0},{9,15},{... | collective-permute-start | bytes 1179656 | tf_op jit(solution)/shard_map/ppermute | solution.py:64
  119.2 1.4 collective-permute-start.24
  120.6 2.2 %shard_map.151 = (bf16[256,2048]{1,0:T(8,128)(2,1)}, bf16[256,2048]{1,0:T(8,128)(2,1)S(1)}) custom-call(bf16[256,2048]{1,0:T(8,128)(2,1)S(1)} %collective-permute-done.1.rows_in.refs_0_, bf16[256,2048]{1,0:T(8,128)(2,1)S(1)} %shard_map.144.refs_1_, bf16[256,2048]{1,0:T(8,128)(2,1)S(1)} %collective-permute-done.44.refs_2_, f32[1,2048]{1,0:T(1,128)S(1)} %bitcast.14), custom_call_target="tpu_custom_call" | custom-call | flops 1048576 | bytes 4194304 | tf_op jit(solution)/shard_map/pallas_call | solution.py:289
  123.9 3.5 %collective-permute-done.33.refs_1_ = bf16[512,768]{1,0:T(8,128)(2,1)S(1)} collective-permute-done((bf16[512,768]{1,0:T(8,128)(2,1)S(1)}, bf16[512,768]{1,0:T(8,128)(2,1)S(1)}, u32[]{:S(2)}, u32[]{:S(2)}) %collective-permute-start.33) | collective-permute-done | bytes 786464 | tf_op jit(solution)/shard_map/ppermute | solution.py:64
  127.4 4.2 %collective-permute-done.42.refs_3_ = bf16[256,768]{1,0:T(8,128)(2,1)S(1)} collective-permute-done((bf16[256,768]{1,0:T(8,128)(2,1)S(1)}, bf16[256,768]{1,0:T(8,128)(2,1)S(1)}, u32[]{:S(2)}, u32[]{:S(2)}) %collective-permute-start.42) | collective-permute-done | bytes 393248 | tf_op jit(solution)/shard_map/ppermute | solution.py:64
  133.1 6.7 %collective-permute-done.38.refs_7_ = bf16[512,768]{1,0:T(8,128)(2,1)S(1)} collective-permute-done((bf16[512,768]{1,0:T(8,128)(2,1)S(1)}, bf16[512,768]{1,0:T(8,128)(2,1)S(1)}, u32[]{:S(2)}, u32[]{:S(2)}) %collective-permute-start.38) | collective-permute-done | bytes 786464 | tf_op jit(solution)/shard_map/ppermute | solution.py:64
  139.8 8.4 %collective-permute-done.35.refs_2_ = bf16[512,768]{1,0:T(8,128)(2,1)S(1)} collective-permute-done((bf16[512,768]{1,0:T(8,128)(2,1)S(1)}, bf16[512,768]{1,0:T(8,128)(2,1)S(1)}, u32[]{:S(2)}, u32[]{:S(2)}) %collective-permute-start.35) | collective-permute-done | bytes 786464 | tf_op jit(solution)/shard_map/ppermute | solution.py:64
  148.7 1.4 shard_map.145
  150.1 3.3 %collective-permute-start.25 = (bf16[256,2048]{1,0:T(8,128)(2,1)S(1)}, bf16[256,2048]{1,0:T(8,128)(2,1)S(1)}, u32[]{:S(2)}, u32[]{:S(2)}) collective-permute-start(bf16[256,2048]{1,0:T(8,128)(2,1)S(1)} %get-tuple-element.36.first), channel_id=1, source_target_pairs={{0,1},{1,0},{2,3},{3,2},{4,5},{5,4},{6,7},{7,6},{8,9},{9,8},{10,11... | collective-permute-start | bytes 3145736 | tf_op jit(solution)/shard_map/ppermute | solution.py:36
  153.4 3.7 %shard_map.152.hidden = bf16[2,256,768]{2,1,0:T(8,128)(2,1)S(1)} custom-call(bf16[256,2048]{1,0:T(8,128)(2,1)S(1)} %get-tuple-element.44.first, bf16[256,2048]{1,0:T(8,128)(2,1)S(1)} %collective-permute-done.45.second, bf16[2048,768]{1,0:T(8,128)(2,1)S(1)} %get-tuple-element.39.wgate, bf16[2048,768]{1,0:T(8,128)(2,1)S(1)} %get-tuple-element.40.wup, ...), custom_call_target="tpu_custom_call" | custom-call | flops 3221225472 | bytes 8388608 | tf_op jit(solution)/shard_map/pallas_call | solution.py:260
  157.1 1.8 %shard_map.153 = (bf16[256,2048]{1,0:T(8,128)(2,1)S(1)}, bf16[256,2048]{1,0:T(8,128)(2,1)S(1)}) custom-call(bf16[2,256,768]{2,1,0:T(8,128)(2,1)S(1)} %shard_map.152.hidden, bf16[2048,768]{1,0:T(8,128)(2,1)S(1)} %shard_map.149.wdown), custom_call_target="tpu_custom_call" | custom-call | flops 1610612736 | bytes 8388608 | tf_op jit(solution)/shard_map/pallas_call | solution.py:260
  159.1 3.8 %shard_map.148.hidden = bf16[2,256,768]{2,1,0:T(8,128)(2,1)S(1)} custom-call(bf16[256,2048]{1,0:T(8,128)(2,1)S(1)} %get-tuple-element.36.first, bf16[256,2048]{1,0:T(8,128)(2,1)S(1)} %collective-permute-done.25.second, bf16[2048,768]{1,0:T(8,128)(2,1)S(1)} %get-tuple-element.39.wgate, bf16[2048,768]{1,0:T(8,128)(2,1)S(1)} %get-tuple-element.40.wup, ...), custom_call_target="tpu_custom_call" | custom-call | flops 3221225472 | bytes 8388608 | tf_op jit(solution)/shard_map/pallas_call | solution.py:260
  162.8 1.8 %shard_map.150 = (bf16[256,2048]{1,0:T(8,128)(2,1)S(1)}, bf16[256,2048]{1,0:T(8,128)(2,1)S(1)}) custom-call(bf16[2,256,768]{2,1,0:T(8,128)(2,1)S(1)} %shard_map.148.hidden, bf16[2048,768]{1,0:T(8,128)(2,1)S(1)} %shard_map.149.wdown), custom_call_target="tpu_custom_call" | custom-call | flops 1610612736 | bytes 8388608 | tf_op jit(solution)/shard_map/pallas_call | solution.py:260
  165.6 1.9 %collective-permute-done.43.refs_2_ = bf16[256,2048]{1,0:T(8,128)(2,1)S(1)} collective-permute-done((bf16[256,2048]{1,0:T(8,128)(2,1)S(1)}, bf16[256,2048]{1,0:T(8,128)(2,1)S(1)}, u32[]{:S(2)}, u32[]{:S(2)}) %collective-permute-start.43) | collective-permute-done | bytes 1048608 | tf_op jit(solution)/shard_map/ppermute | solution.py:36
  167.5 12.0 %collective-permute-done.47.refs_3_ = bf16[256,2048]{1,0:T(8,128)(2,1)S(1)} collective-permute-done((bf16[256,2048]{1,0:T(8,128)(2,1)S(1)}, bf16[256,2048]{1,0:T(8,128)(2,1)S(1)}, u32[]{:S(2)}, u32[]{:S(2)}) %collective-permute-start.47) | collective-permute-done | bytes 1048608 | tf_op jit(solution)/shard_map/ppermute | solution.py:52
  179.5 1.5 shard_map.155
  (113 shorter events, 18.6 us)
Async XLA Ops:
  0.0 33.5 %collective-permute-start.1 = (bf16[256,2048]{1,0:T(8,128)(2,1)}, bf16[256,2048]{1,0:T(8,128)(2,1)S(1)}, u32[]{:S(2)}, u32[]{:S(2)}) collective-permute-start(bf16[256,2048]{1,0:T(8,128)(2,1)} %refs_0_.1), channel_id=1, source_target_pairs={{0,96},{1,33},{32,0},{33,65},{64,32},{65,97},{96,64},{97,1},{2,98}... | collective-permute-start | bytes 3145736 | tf_op jit(solution)/shard_map/ppermute | solution.py:44
  4.3 7.2 %collective-permute-start.3 = (bf16[64,1536]{1,0:T(8,128)(2,1)S(1)}, bf16[64,1536]{1,0:T(8,128)(2,1)S(1)}, u32[]{:S(2)}, u32[]{:S(2)}) collective-permute-start(bf16[64,1536]{1,0:T(8,128)(2,1)S(1)} %pad_maximum_fusion.3), channel_id=1, source_target_pairs={{0,32},{1,97},{32,64},{33,1},{64,96},{65,33},{96,0},{97,65},{2,34}... | collective-permute-start | bytes 589832 | tf_op jit(solution)/shard_map/ppermute | solution.py:52
  6.7 7.6 %collective-permute-start.4 = (bf16[64,1536]{1,0:T(8,128)(2,1)S(1)}, bf16[64,1536]{1,0:T(8,128)(2,1)S(1)}, u32[]{:S(2)}, u32[]{:S(2)}) collective-permute-start(bf16[64,1536]{1,0:T(8,128)(2,1)S(1)} %pad_maximum_fusion.2.refs_0_), channel_id=1, source_target_pairs={{0,6},{1,25},{2,0},{3,27},{4,2},{5,29},{6,4},{7,31},{8,14},{9,1},{... | collective-permute-start | bytes 589832 | tf_op jit(solution)/shard_map/ppermute | solution.py:64
  9.5 6.4 %collective-permute-start.6 = (bf16[64,1536]{1,0:T(8,128)(2,1)S(1)}, bf16[64,1536]{1,0:T(8,128)(2,1)S(1)}, u32[]{:S(2)}, u32[]{:S(2)}) collective-permute-start(bf16[64,1536]{1,0:T(8,128)(2,1)S(1)} %pad_maximum_fusion.2.refs_0_), channel_id=1, source_target_pairs={{0,4},{1,17},{2,6},{3,19},{4,0},{5,21},{6,2},{7,23},{8,12},{9,25},... | collective-permute-start | bytes 589832 | tf_op jit(solution)/shard_map/ppermute | solution.py:64
  9.8 8.4 %collective-permute-start.8 = (bf16[64,1536]{1,0:T(8,128)(2,1)S(1)}, bf16[64,1536]{1,0:T(8,128)(2,1)S(1)}, u32[]{:S(2)}, u32[]{:S(2)}) collective-permute-start(bf16[64,1536]{1,0:T(8,128)(2,1)S(1)} %pad_maximum_fusion.2.refs_0_), channel_id=1, source_target_pairs={{0,2},{1,9},{2,4},{3,11},{4,6},{5,13},{6,0},{7,15},{8,10},{9,17},{... | collective-permute-start | bytes 589832 | tf_op jit(solution)/shard_map/ppermute | solution.py:64
  11.5 6.7 %collective-permute-start.5 = (bf16[64,1536]{1,0:T(8,128)(2,1)S(1)}, bf16[64,1536]{1,0:T(8,128)(2,1)S(1)}, u32[]{:S(2)}, u32[]{:S(2)}) collective-permute-start(bf16[64,1536]{1,0:T(8,128)(2,1)S(1)} %collective-permute-done.3.refs_1_), channel_id=1, source_target_pairs={{0,6},{1,25},{2,0},{3,27},{4,2},{5,29},{6,4},{7,31},{8,14},{9,1},{... | collective-permute-start | bytes 589832 | tf_op jit(solution)/shard_map/ppermute | solution.py:64
  14.2 6.1 %collective-permute-start.7 = (bf16[64,1536]{1,0:T(8,128)(2,1)S(1)}, bf16[64,1536]{1,0:T(8,128)(2,1)S(1)}, u32[]{:S(2)}, u32[]{:S(2)}) collective-permute-start(bf16[64,1536]{1,0:T(8,128)(2,1)S(1)} %collective-permute-done.3.refs_1_), channel_id=1, source_target_pairs={{0,4},{1,17},{2,6},{3,19},{4,0},{5,21},{6,2},{7,23},{8,12},{9,25},... | collective-permute-start | bytes 589832 | tf_op jit(solution)/shard_map/ppermute | solution.py:64
  15.8 6.5 %collective-permute-start.9 = (bf16[64,1536]{1,0:T(8,128)(2,1)S(1)}, bf16[64,1536]{1,0:T(8,128)(2,1)S(1)}, u32[]{:S(2)}, u32[]{:S(2)}) collective-permute-start(bf16[64,1536]{1,0:T(8,128)(2,1)S(1)} %collective-permute-done.3.refs_1_), channel_id=1, source_target_pairs={{0,2},{1,9},{2,4},{3,11},{4,6},{5,13},{6,0},{7,15},{8,10},{9,17},{... | collective-permute-start | bytes 589832 | tf_op jit(solution)/shard_map/ppermute | solution.py:64
  23.7 11.9 %collective-permute-start.14 = (bf16[512,512]{1,0:T(8,128)(2,1)}, bf16[512,512]{1,0:T(8,128)(2,1)}, u32[]{:S(2)}, u32[]{:S(2)}) collective-permute-start(bf16[512,512]{1,0:T(8,128)(2,1)} %get-tuple-element.27.rest_0_), channel_id=1, source_target_pairs={{0,8},{1,3},{2,10},{3,5},{4,12},{5,7},{6,14},{7,1},{8,16},{9,11},{... | collective-permute-start | bytes 1572872 | tf_op jit(solution)/shard_map/ppermute | solution.py:64
  26.0 23.7 %collective-permute-start = (bf16[256,2048]{1,0:T(8,128)(2,1)S(1)}, bf16[256,2048]{1,0:T(8,128)(2,1)}, u32[]{:S(2)}, u32[]{:S(2)}) collective-permute-start(bf16[256,2048]{1,0:T(8,128)(2,1)S(1)} %shard_map.136.own), channel_id=1, source_target_pairs={{0,1},{1,0},{2,3},{3,2},{4,5},{5,4},{6,7},{7,6},{8,9},{9,8},{10,11... | collective-permute-start | bytes 3145736 | tf_op jit(solution)/shard_map/ppermute | solution.py:36
  35.6 16.9 %collective-permute-start.2 = (bf16[256,2048]{1,0:T(8,128)(2,1)}, bf16[256,2048]{1,0:T(8,128)(2,1)}, u32[]{:S(2)}, u32[]{:S(2)}) collective-permute-start(bf16[256,2048]{1,0:T(8,128)(2,1)} %shard_map.137.rem), channel_id=1, source_target_pairs={{0,1},{1,0},{2,3},{3,2},{4,5},{5,4},{6,7},{7,6},{8,9},{9,8},{10,11... | collective-permute-start | bytes 3145736 | tf_op jit(solution)/shard_map/ppermute | solution.py:36
  35.6 8.5 %collective-permute-start.13 = (bf16[512,512]{1,0:T(8,128)(2,1)}, bf16[512,512]{1,0:T(8,128)(2,1)S(1)}, u32[]{:S(2)}, u32[]{:S(2)}) collective-permute-start(bf16[512,512]{1,0:T(8,128)(2,1)} %get-tuple-element.27.rest_0_), channel_id=1, source_target_pairs={{0,24},{1,7},{2,26},{3,1},{4,28},{5,3},{6,30},{7,5},{8,0},{9,15},{... | collective-permute-start | bytes 1572872 | tf_op jit(solution)/shard_map/ppermute | solution.py:64
  35.6 14.2 %collective-permute-start.10 = (bf16[512,512]{1,0:T(8,128)(2,1)}, bf16[512,512]{1,0:T(8,128)(2,1)S(1)}, u32[]{:S(2)}, u32[]{:S(2)}) collective-permute-start(bf16[512,512]{1,0:T(8,128)(2,1)} %copy-done.4), channel_id=1, source_target_pairs={{0,24},{1,7},{2,26},{3,1},{4,28},{5,3},{6,30},{7,5},{8,0},{9,15},{... | collective-permute-start | bytes 1572872 | tf_op jit(solution)/shard_map/ppermute | solution.py:64
  35.6 16.8 %collective-permute-start.15 = (bf16[512,512]{1,0:T(8,128)(2,1)}, bf16[512,512]{1,0:T(8,128)(2,1)S(1)}, u32[]{:S(2)}, u32[]{:S(2)}) collective-permute-start(bf16[512,512]{1,0:T(8,128)(2,1)} %collective-permute-done.14.rest_3_), channel_id=1, source_target_pairs={{0,8},{1,3},{2,10},{3,5},{4,12},{5,7},{6,14},{7,1},{8,16},{9,11},{... | collective-permute-start | bytes 1572872 | tf_op jit(solution)/shard_map/ppermute | solution.py:64
  44.1 24.5 %collective-permute-start.26 = (bf16[64,2304]{1,0:T(8,128)(2,1)S(1)}, bf16[64,2304]{1,0:T(8,128)(2,1)S(1)}, u32[]{:S(2)}, u32[]{:S(2)}) collective-permute-start(bf16[64,2304]{1,0:T(8,128)(2,1)S(1)} %pad_maximum_fusion.1), channel_id=1, source_target_pairs={{0,32},{1,97},{32,64},{33,1},{64,96},{65,33},{96,0},{97,65},{2,34}... | collective-permute-start | bytes 884744 | tf_op jit(solution)/shard_map/ppermute | solution.py:52
  49.8 11.6 %collective-permute-start.12 = (bf16[512,512]{1,0:T(8,128)(2,1)}, bf16[512,512]{1,0:T(8,128)(2,1)S(1)}, u32[]{:S(2)}, u32[]{:S(2)}) collective-permute-start(bf16[512,512]{1,0:T(8,128)(2,1)} %copy-done.4), channel_id=1, source_target_pairs={{0,8},{1,3},{2,10},{3,5},{4,12},{5,7},{6,14},{7,1},{8,16},{9,11},{... | collective-permute-start | bytes 1572872 | tf_op jit(solution)/shard_map/ppermute | solution.py:64
  49.8 12.4 %collective-permute-start.11 = (bf16[512,512]{1,0:T(8,128)(2,1)S(1)}, bf16[512,512]{1,0:T(8,128)(2,1)S(1)}, u32[]{:S(2)}, u32[]{:S(2)}) collective-permute-start(bf16[512,512]{1,0:T(8,128)(2,1)S(1)} %collective-permute-done.10.rest_1_), channel_id=1, source_target_pairs={{0,24},{1,7},{2,26},{3,1},{4,28},{5,3},{6,30},{7,5},{8,0},{9,15},{... | collective-permute-start | bytes 1572872 | tf_op jit(solution)/shard_map/ppermute | solution.py:64
  57.8 3.4 %collective-permute-start.16 = (f32[4,4,128]{2,1,0:T(4,128)S(1)}, f32[4,4,128]{2,1,0:T(4,128)S(1)}, u32[]{:S(2)}, u32[]{:S(2)}) collective-permute-start(f32[4,4,128]{2,1,0:T(4,128)S(1)} %get-tuple-element.29), channel_id=1, source_target_pairs={{0,1},{1,0},{2,3},{3,2},{4,5},{5,4},{6,7},{7,6},{8,9},{9,8},{10,11... | collective-permute-start | bytes 24584 | tf_op jit(solution)/shard_map/ppermute | solution.py:36
  60.5 12.0 %collective-permute-start.19 = (bf16[512,512]{1,0:T(8,128)(2,1)S(1)}, bf16[512,512]{1,0:T(8,128)(2,1)S(1)}, u32[]{:S(2)}, u32[]{:S(2)}) collective-permute-start(bf16[512,512]{1,0:T(8,128)(2,1)S(1)} %copy-done.3), channel_id=1, source_target_pairs={{0,24},{1,7},{2,26},{3,1},{4,28},{5,3},{6,30},{7,5},{8,0},{9,15},{... | collective-permute-start | bytes 1572872 | tf_op jit(solution)/shard_map/ppermute | solution.py:64
  61.3 11.2 %collective-permute-start.20 = (bf16[512,512]{1,0:T(8,128)(2,1)S(1)}, bf16[512,512]{1,0:T(8,128)(2,1)S(1)}, u32[]{:S(2)}, u32[]{:S(2)}) collective-permute-start(bf16[512,512]{1,0:T(8,128)(2,1)S(1)} %copy-done.3), channel_id=1, source_target_pairs={{0,16},{1,5},{2,18},{3,7},{4,20},{5,1},{6,22},{7,3},{8,24},{9,13},... | collective-permute-start | bytes 1572872 | tf_op jit(solution)/shard_map/ppermute | solution.py:64
  61.4 16.5 %collective-permute-start.21 = (bf16[512,512]{1,0:T(8,128)(2,1)S(1)}, bf16[512,512]{1,0:T(8,128)(2,1)S(1)}, u32[]{:S(2)}, u32[]{:S(2)}) collective-permute-start(bf16[512,512]{1,0:T(8,128)(2,1)S(1)} %copy-done.3), channel_id=1, source_target_pairs={{0,8},{1,3},{2,10},{3,5},{4,12},{5,7},{6,14},{7,1},{8,16},{9,11},{... | collective-permute-start | bytes 1572872 | tf_op jit(solution)/shard_map/ppermute | solution.py:64
  62.2 4.9 %collective-permute-start.18 = (f32[2,4,128]{2,1,0:T(4,128)S(1)}, f32[2,4,128]{2,1,0:T(4,128)S(1)}, u32[]{:S(2)}, u32[]{:S(2)}) collective-permute-start(f32[2,4,128]{2,1,0:T(4,128)S(1)} %pad_maximum_fusion.4), channel_id=1, source_target_pairs={{0,96},{32,0},{64,32},{96,64},{1,97},{33,1},{65,33},{97,65},{2,98}... | collective-permute-start | bytes 12296 | tf_op jit(solution)/shard_map/ppermute | solution.py:32
  67.1 4.0 %collective-permute-start.17 = (f32[2,4,128]{2,1,0:T(4,128)S(1)}, f32[2,4,128]{2,1,0:T(4,128)S(1)}, u32[]{:S(2)}, u32[]{:S(2)}) collective-permute-start(f32[2,4,128]{2,1,0:T(4,128)S(1)} %slice.36), channel_id=1, source_target_pairs={{0,32},{32,64},{64,96},{96,0},{1,33},{33,65},{65,97},{97,1},{2,34}... | collective-permute-start | bytes 12296 | tf_op jit(solution)/shard_map/ppermute | solution.py:32
  68.6 17.1 %collective-permute-start.29 = (bf16[64,2304]{1,0:T(8,128)(2,1)S(1)}, bf16[64,2304]{1,0:T(8,128)(2,1)S(1)}, u32[]{:S(2)}, u32[]{:S(2)}) collective-permute-start(bf16[64,2304]{1,0:T(8,128)(2,1)S(1)} %pad_maximum_fusion.refs_0_), channel_id=1, source_target_pairs={{0,2},{1,9},{2,4},{3,11},{4,6},{5,13},{6,0},{7,15},{8,10},{9,17},{... | collective-permute-start | bytes 884744 | tf_op jit(solution)/shard_map/ppermute | solution.py:64
  71.1 14.6 %collective-permute-start.28 = (bf16[64,2304]{1,0:T(8,128)(2,1)S(1)}, bf16[64,2304]{1,0:T(8,128)(2,1)S(1)}, u32[]{:S(2)}, u32[]{:S(2)}) collective-permute-start(bf16[64,2304]{1,0:T(8,128)(2,1)S(1)} %collective-permute-done.26.refs_1_), channel_id=1, source_target_pairs={{0,6},{1,25},{2,0},{3,27},{4,2},{5,29},{6,4},{7,31},{8,14},{9,1},{... | collective-permute-start | bytes 884744 | tf_op jit(solution)/shard_map/ppermute | solution.py:64
  80.3 21.6 %collective-permute-start.22 = (bf16[256,2048]{1,0:T(8,128)(2,1)S(1)}, bf16[256,2048]{1,0:T(8,128)(2,1)S(1)}, u32[]{:S(2)}, u32[]{:S(2)}) collective-permute-start(bf16[256,2048]{1,0:T(8,128)(2,1)S(1)} %get-tuple-element.32), channel_id=1, source_target_pairs={{0,1},{1,0},{2,3},{3,2},{4,5},{5,4},{6,7},{7,6},{8,9},{9,8},{10,11... | collective-permute-start | bytes 3145736 | tf_op jit(solution)/shard_map/ppermute | solution.py:36
  84.2 5.9 %collective-permute-start.27 = (bf16[64,2304]{1,0:T(8,128)(2,1)S(1)}, bf16[64,2304]{1,0:T(8,128)(2,1)S(1)}, u32[]{:S(2)}, u32[]{:S(2)}) collective-permute-start(bf16[64,2304]{1,0:T(8,128)(2,1)S(1)} %pad_maximum_fusion.refs_0_), channel_id=1, source_target_pairs={{0,6},{1,25},{2,0},{3,27},{4,2},{5,29},{6,4},{7,31},{8,14},{9,1},{... | collective-permute-start | bytes 884744 | tf_op jit(solution)/shard_map/ppermute | solution.py:64
  84.5 10.2 %collective-permute-start.32 = (bf16[64,2304]{1,0:T(8,128)(2,1)S(1)}, bf16[64,2304]{1,0:T(8,128)(2,1)S(1)}, u32[]{:S(2)}, u32[]{:S(2)}) collective-permute-start(bf16[64,2304]{1,0:T(8,128)(2,1)S(1)} %collective-permute-done.26.refs_1_), channel_id=1, source_target_pairs={{0,2},{1,9},{2,4},{3,11},{4,6},{5,13},{6,0},{7,15},{8,10},{9,17},{... | collective-permute-start | bytes 884744 | tf_op jit(solution)/shard_map/ppermute | solution.py:64
  85.7 9.1 %collective-permute-start.30 = (bf16[64,2304]{1,0:T(8,128)(2,1)S(1)}, bf16[64,2304]{1,0:T(8,128)(2,1)S(1)}, u32[]{:S(2)}, u32[]{:S(2)}) collective-permute-start(bf16[64,2304]{1,0:T(8,128)(2,1)S(1)} %collective-permute-done.29.refs_6_), channel_id=1, source_target_pairs={{0,2},{1,9},{2,4},{3,11},{4,6},{5,13},{6,0},{7,15},{8,10},{9,17},{... | collective-permute-start | bytes 884744 | tf_op jit(solution)/shard_map/ppermute | solution.py:64
  85.7 9.1 %collective-permute-start.31 = (bf16[64,2304]{1,0:T(8,128)(2,1)S(1)}, bf16[64,2304]{1,0:T(8,128)(2,1)S(1)}, u32[]{:S(2)}, u32[]{:S(2)}) collective-permute-start(bf16[64,2304]{1,0:T(8,128)(2,1)S(1)} %collective-permute-done.28.refs_3_), channel_id=1, source_target_pairs={{0,6},{1,25},{2,0},{3,27},{4,2},{5,29},{6,4},{7,31},{8,14},{9,1},{... | collective-permute-start | bytes 884744 | tf_op jit(solution)/shard_map/ppermute | solution.py:64
  95.4 12.4 %collective-permute-start.40 = (bf16[512,768]{1,0:T(8,128)(2,1)S(1)}, bf16[512,768]{1,0:T(8,128)(2,1)S(1)}, u32[]{:S(2)}, u32[]{:S(2)}) collective-permute-start(bf16[512,768]{1,0:T(8,128)(2,1)S(1)} %get-tuple-element.41.refs_0_), channel_id=1, source_target_pairs={{0,8},{1,3},{2,10},{3,5},{4,12},{5,7},{6,14},{7,1},{8,16},{9,11},{... | collective-permute-start | bytes 2359304 | tf_op jit(solution)/shard_map/ppermute | solution.py:64
  95.5 12.3 %collective-permute-start.39 = (bf16[512,768]{1,0:T(8,128)(2,1)S(1)}, bf16[512,768]{1,0:T(8,128)(2,1)S(1)}, u32[]{:S(2)}, u32[]{:S(2)}) collective-permute-start(bf16[512,768]{1,0:T(8,128)(2,1)S(1)} %get-tuple-element.41.refs_0_), channel_id=1, source_target_pairs={{0,24},{1,7},{2,26},{3,1},{4,28},{5,3},{6,30},{7,5},{8,0},{9,15},{... | collective-permute-start | bytes 2359304 | tf_op jit(solution)/shard_map/ppermute | solution.py:64
  100.6 15.6 %collective-permute-start.23 = (bf16[256,2048]{1,0:T(8,128)(2,1)S(1)}, bf16[256,2048]{1,0:T(8,128)(2,1)S(1)}, u32[]{:S(2)}, u32[]{:S(2)}) collective-permute-start(bf16[256,2048]{1,0:T(8,128)(2,1)S(1)} %get-tuple-element.34), channel_id=1, source_target_pairs={{0,1},{1,0},{2,3},{3,2},{4,5},{5,4},{6,7},{7,6},{8,9},{9,8},{10,11... | collective-permute-start | bytes 3145736 | tf_op jit(solution)/shard_map/ppermute | solution.py:36
  102.3 17.0 %collective-permute-start.44 = (bf16[256,2048]{1,0:T(8,128)(2,1)S(1)}, bf16[256,2048]{1,0:T(8,128)(2,1)S(1)}, u32[]{:S(2)}, u32[]{:S(2)}) collective-permute-start(bf16[256,2048]{1,0:T(8,128)(2,1)S(1)} %shard_map.142.refs_1_), channel_id=1, source_target_pairs={{0,96},{1,33},{32,0},{33,65},{64,32},{65,97},{96,64},{97,1},{2,98}... | collective-permute-start | bytes 3145736 | tf_op jit(solution)/shard_map/ppermute | solution.py:44
  102.3 13.9 %collective-permute-start.34 = (bf16[512,768]{1,0:T(8,128)(2,1)S(1)}, bf16[512,768]{1,0:T(8,128)(2,1)S(1)}, u32[]{:S(2)}, u32[]{:S(2)}) collective-permute-start(bf16[512,768]{1,0:T(8,128)(2,1)S(1)} %get-tuple-element.37.refs_0_), channel_id=1, source_target_pairs={{0,8},{1,3},{2,10},{3,5},{4,12},{5,7},{6,14},{7,1},{8,16},{9,11},{... | collective-permute-start | bytes 2359304 | tf_op jit(solution)/shard_map/ppermute | solution.py:64
  107.8 15.0 %collective-permute-start.36 = (bf16[512,768]{1,0:T(8,128)(2,1)S(1)}, bf16[512,768]{1,0:T(8,128)(2,1)S(1)}, u32[]{:S(2)}, u32[]{:S(2)}) collective-permute-start(bf16[512,768]{1,0:T(8,128)(2,1)S(1)} %get-tuple-element.38.refs_4_), channel_id=1, source_target_pairs={{0,24},{1,7},{2,26},{3,1},{4,28},{5,3},{6,30},{7,5},{8,0},{9,15},{... | collective-permute-start | bytes 2359304 | tf_op jit(solution)/shard_map/ppermute | solution.py:64
  107.8 19.6 %collective-permute-start.33 = (bf16[512,768]{1,0:T(8,128)(2,1)S(1)}, bf16[512,768]{1,0:T(8,128)(2,1)S(1)}, u32[]{:S(2)}, u32[]{:S(2)}) collective-permute-start(bf16[512,768]{1,0:T(8,128)(2,1)S(1)} %get-tuple-element.37.refs_0_), channel_id=1, source_target_pairs={{0,24},{1,7},{2,26},{3,1},{4,28},{5,3},{6,30},{7,5},{8,0},{9,15},{... | collective-permute-start | bytes 2359304 | tf_op jit(solution)/shard_map/ppermute | solution.py:64
  116.3 11.1 %collective-permute-start.41 = (bf16[256,768]{1,0:T(8,128)(2,1)S(1)}, bf16[256,768]{1,0:T(8,128)(2,1)S(1)}, u32[]{:S(2)}, u32[]{:S(2)}) collective-permute-start(bf16[256,768]{1,0:T(8,128)(2,1)S(1)} %slice.43), channel_id=1, source_target_pairs={{0,8},{1,3},{2,10},{3,5},{4,12},{5,7},{6,14},{7,1},{8,16},{9,11},{... | collective-permute-start | bytes 1179656 | tf_op jit(solution)/shard_map/ppermute | solution.py:64
  116.3 15.3 %collective-permute-start.42 = (bf16[256,768]{1,0:T(8,128)(2,1)S(1)}, bf16[256,768]{1,0:T(8,128)(2,1)S(1)}, u32[]{:S(2)}, u32[]{:S(2)}) collective-permute-start(bf16[256,768]{1,0:T(8,128)(2,1)S(1)} %slice.44), channel_id=1, source_target_pairs={{0,24},{1,7},{2,26},{3,1},{4,28},{5,3},{6,30},{7,5},{8,0},{9,15},{... | collective-permute-start | bytes 1179656 | tf_op jit(solution)/shard_map/ppermute | solution.py:64
  119.2 29.4 %collective-permute-start.24 = (bf16[256,2048]{1,0:T(8,128)(2,1)S(1)}, bf16[256,2048]{1,0:T(8,128)(2,1)S(1)}, u32[]{:S(2)}, u32[]{:S(2)}) collective-permute-start(bf16[256,2048]{1,0:T(8,128)(2,1)S(1)} %shard_map.144.refs_1_), channel_id=1, source_target_pairs={{0,32},{1,97},{32,64},{33,1},{64,96},{65,33},{96,0},{97,65},{2,34}... | collective-permute-start | bytes 3145736 | tf_op jit(solution)/shard_map/ppermute | solution.py:52
  122.9 30.5 %collective-permute-start.45 = (bf16[256,2048]{1,0:T(8,128)(2,1)S(1)}, bf16[256,2048]{1,0:T(8,128)(2,1)S(1)}, u32[]{:S(2)}, u32[]{:S(2)}) collective-permute-start(bf16[256,2048]{1,0:T(8,128)(2,1)S(1)} %get-tuple-element.44.first), channel_id=1, source_target_pairs={{0,1},{1,0},{2,3},{3,2},{4,5},{5,4},{6,7},{7,6},{8,9},{9,8},{10,11... | collective-permute-start | bytes 3145736 | tf_op jit(solution)/shard_map/ppermute | solution.py:36
  127.4 12.3 %collective-permute-start.38 = (bf16[512,768]{1,0:T(8,128)(2,1)S(1)}, bf16[512,768]{1,0:T(8,128)(2,1)S(1)}, u32[]{:S(2)}, u32[]{:S(2)}) collective-permute-start(bf16[512,768]{1,0:T(8,128)(2,1)S(1)} %get-tuple-element.38.refs_4_), channel_id=1, source_target_pairs={{0,8},{1,3},{2,10},{3,5},{4,12},{5,7},{6,14},{7,1},{8,16},{9,11},{... | collective-permute-start | bytes 2359304 | tf_op jit(solution)/shard_map/ppermute | solution.py:64
  127.4 20.8 %collective-permute-start.35 = (bf16[512,768]{1,0:T(8,128)(2,1)S(1)}, bf16[512,768]{1,0:T(8,128)(2,1)S(1)}, u32[]{:S(2)}, u32[]{:S(2)}) collective-permute-start(bf16[512,768]{1,0:T(8,128)(2,1)S(1)} %collective-permute-done.34.refs_3_), channel_id=1, source_target_pairs={{0,8},{1,3},{2,10},{3,5},{4,12},{5,7},{6,14},{7,1},{8,16},{9,11},{... | collective-permute-start | bytes 2359304 | tf_op jit(solution)/shard_map/ppermute | solution.py:64
  131.6 16.6 %collective-permute-start.37 = (bf16[512,768]{1,0:T(8,128)(2,1)S(1)}, bf16[512,768]{1,0:T(8,128)(2,1)S(1)}, u32[]{:S(2)}, u32[]{:S(2)}) collective-permute-start(bf16[512,768]{1,0:T(8,128)(2,1)S(1)} %collective-permute-done.36.refs_5_), channel_id=1, source_target_pairs={{0,24},{1,7},{2,26},{3,1},{4,28},{5,3},{6,30},{7,5},{8,0},{9,15},{... | collective-permute-start | bytes 2359304 | tf_op jit(solution)/shard_map/ppermute | solution.py:64
  150.1 9.0 %collective-permute-start.25 = (bf16[256,2048]{1,0:T(8,128)(2,1)S(1)}, bf16[256,2048]{1,0:T(8,128)(2,1)S(1)}, u32[]{:S(2)}, u32[]{:S(2)}) collective-permute-start(bf16[256,2048]{1,0:T(8,128)(2,1)S(1)} %get-tuple-element.36.first), channel_id=1, source_target_pairs={{0,1},{1,0},{2,3},{3,2},{4,5},{5,4},{6,7},{7,6},{8,9},{9,8},{10,11... | collective-permute-start | bytes 3145736 | tf_op jit(solution)/shard_map/ppermute | solution.py:36
  159.0 6.3 %collective-permute-start.46 = (bf16[256,2048]{1,0:T(8,128)(2,1)S(1)}, bf16[256,2048]{1,0:T(8,128)(2,1)S(1)}, u32[]{:S(2)}, u32[]{:S(2)}) collective-permute-start(bf16[256,2048]{1,0:T(8,128)(2,1)S(1)} %get-tuple-element.46), channel_id=1, source_target_pairs={{0,1},{1,0},{2,3},{3,2},{4,5},{5,4},{6,7},{7,6},{8,9},{9,8},{10,11... | collective-permute-start | bytes 3145736 | tf_op jit(solution)/shard_map/ppermute | solution.py:36
  164.7 2.8 %collective-permute-start.43 = (bf16[256,2048]{1,0:T(8,128)(2,1)S(1)}, bf16[256,2048]{1,0:T(8,128)(2,1)S(1)}, u32[]{:S(2)}, u32[]{:S(2)}) collective-permute-start(bf16[256,2048]{1,0:T(8,128)(2,1)S(1)} %get-tuple-element.43), channel_id=1, source_target_pairs={{0,1},{1,0},{2,3},{3,2},{4,5},{5,4},{6,7},{7,6},{8,9},{9,8},{10,11... | collective-permute-start | bytes 3145736 | tf_op jit(solution)/shard_map/ppermute | solution.py:36
  165.5 14.0 %collective-permute-start.47 = (bf16[256,2048]{1,0:T(8,128)(2,1)S(1)}, bf16[256,2048]{1,0:T(8,128)(2,1)S(1)}, u32[]{:S(2)}, u32[]{:S(2)}) collective-permute-start(bf16[256,2048]{1,0:T(8,128)(2,1)S(1)} %shard_map.154), channel_id=1, source_target_pairs={{0,32},{1,97},{32,64},{33,1},{64,96},{65,33},{96,0},{97,65},{2,34}... | collective-permute-start | bytes 3145736 | tf_op jit(solution)/shard_map/ppermute | solution.py:52
  (14 other events, 260.9 us)
